TPU v7x, 32 devices: a whole 2x2x4 slice. The times are simulated.
32 devices in a mesh: sp: 8 (over z, x), tp: 4 (over y, core).
Axes of the slice: x: 2, y: 2, z: 4, core: 2. Of those that a mesh axis runs over, the one named last changes fastest.
Arguments:
- latent: bfloat16 [2, 4096, 2048], P(None, ('sp', 'tp')), may hold values from -6 to 6
- context: bfloat16 [2, 512, 2048], P(None, 'sp'), may hold values from -6 to 6
- cond: bfloat16 [2, 2048], replicated, may hold values from -6 to 6
- ctx_cond: bfloat16 [2048], replicated, may hold values from -6 to 6
- w_shift: bfloat16 [2048, 2048], P('sp', 'tp'), may hold values from -0.125 to 0.125
- w_scale: bfloat16 [2048, 2048], P('sp', 'tp'), may hold values from -0.125 to 0.125
- w_gate: bfloat16 [2048, 2048], P('sp', 'tp'), may hold values from -0.125 to 0.125
- norm_gain: float32 [2048], replicated, may hold values from 0.1 to 1.9
- w_query: bfloat16 [2048, 2048], P(None, 'tp'), may hold values from -1.08275726 to 1.08275726
- w_key: bfloat16 [2048, 2048], P(None, 'tp'), may hold values from -0.090598056 to 0.090598056
- w_value: bfloat16 [2048, 2048], P(None, 'tp'), may hold values from -0.125 to 0.125
- w_out: bfloat16 [2048, 2048], P('tp'), may hold values from -1.5 to 1.5
- rel_bias: float32 [32, 15, 31], P('tp'), may hold values from -4 to 4
- ctx_bias: float32 [32], P('tp'), may hold values from -3.5 to -2
Outputs:
- mixed: bfloat16 [2, 4096, 2048], P(None, ('sp', 'tp'))
All inputs are finite; a program needn't handle non-finite values.
Results may differ from a plain program's by a relative error of at most 0.0154.
Values may be sent and summed in bfloat16 or wider, within the bound.
A program may use at most 128 MiB of HBM per device.

v0:
```python
import functools

import jax
import jax.numpy as jnp
from jax import lax
from jax.experimental import pallas as pl
from jax.experimental.pallas import tpu as pltpu
from jax.sharding import PartitionSpec as P

HEAD_DIM = 64
GRID_W = 64
WIN_ROWS = 8
WIN_COLS = 16


EPSILON = 1e-06


def extended(shard, sides, width):
    for axis, dim in sides:
        size, length = (lax.axis_size(axis), shard.shape[dim])
        up = [(i, (i + 1) % size) for i in range(size - 1)]
        down = [(j, i) for i, j in up]
        last = lax.slice_in_dim(shard, length - width, length, axis=dim)
        first = lax.slice_in_dim(shard, 0, width, axis=dim)
        before = lax.ppermute(last, axis, up)
        after = lax.ppermute(first, axis, down)
        shard = jnp.concatenate([before, shard, after], axis=dim)
    return shard


def silu_rows(values):
    return jax.nn.silu(values.astype(jnp.float32)).astype(jnp.bfloat16)


def modulate_rows(rows, gain, shift, scale):
    floats = rows.astype(jnp.float32)
    inverse = lax.rsqrt(jnp.mean(floats * floats, axis=-1, keepdims=True) + EPSILON)
    return (floats * inverse * gain * (1.0 + scale) + shift).astype(jnp.bfloat16)

LOG2E = 1.4426950408889634


def attention_kernel(bias_ref, far_ref, q_ref, k_ref, v_ref, ck_ref, cv_ref, out_ref, table):
    pair = pl.program_id(0)
    rows_dev = q_ref.shape[1]
    padded = k_ref.shape[1]
    span = 2 * WIN_COLS
    half = WIN_COLS // 2
    reach = WIN_ROWS // 2
    nq, nk = rows_dev * WIN_COLS, padded * span
    lanes = 2 * HEAD_DIM

    @pl.when(pl.program_id(1) == 0)
    def _():
        sp = lax.axis_index("sp")
        rows_all = rows_dev * lax.axis_size("sp")
        at = lax.broadcasted_iota(jnp.int32, (WIN_COLS, nk), 1)
        p = lax.broadcasted_iota(jnp.int32, (WIN_COLS, nk), 0)
        key_row = sp * rows_dev - reach + at // span
        k = at % span
        inner = (k - p >= 0) & (k - p < WIN_COLS)
        edge = (p < half) == (k < WIN_COLS)
        for r in range(rows_dev):
            row = sp * rows_dev + r
            first = jnp.clip(row - reach, 0, rows_all - WIN_ROWS)
            inside = (key_row >= first) & (key_row < first + WIN_ROWS)
            shift = span * (r + reach - WIN_ROWS + 1) - half + 1
            for h in range(2):
                line = jnp.broadcast_to(bias_ref[0, h : h + 1, :], (WIN_COLS, nk))
                line = pltpu.roll(line, shift % nk, 1, stride=1, stride_axis=0) * LOG2E
                at_rows = pl.ds(r * WIN_COLS, WIN_COLS)
                table[h, 0, at_rows, :] = jnp.where(inside & edge, line, -jnp.inf)
                table[h, 1, at_rows, :] = jnp.where(inside & inner, line, -jnp.inf)

    factor = HEAD_DIM ** (-0.5) * LOG2E
    ck = ck_ref[...].reshape(-1, lanes)
    ctx_count = ck.shape[0]
    cv = jnp.concatenate([cv_ref[...].reshape(-1, lanes), jnp.ones((ctx_count, lanes), jnp.bfloat16)], axis=1)
    ones = jnp.ones((nk, lanes), jnp.bfloat16)
    low = lax.broadcasted_iota(jnp.int32, (nq, lanes), 1) < HEAD_DIM
    contract = (((1,), (1,)), ((), ()))
    every = q_ref[0].astype(jnp.float32)
    outs = []
    for block in range(GRID_W // WIN_COLS):
        if block == 0:
            q = jnp.concatenate([every[:, GRID_W - half :], every[:, :half]], axis=1)
        else:
            q = every[:, WIN_COLS * block - half : WIN_COLS * (block + 1) - half]
        q = q.astype(jnp.bfloat16).reshape(nq, lanes)

        def keys(ref):
            if block == 0:
                got = jnp.concatenate([ref[0, :, GRID_W - WIN_COLS :, :], ref[0, :, :WIN_COLS, :]], 1)
            else:
                got = ref[0, :, WIN_COLS * (block - 1) : WIN_COLS * (block + 1), :]
            return got.reshape(nk, lanes)

        k = keys(k_ref)
        v = jnp.concatenate([keys(v_ref), ones], axis=1)
        halves = []
        for h in range(2):
            mine = low if h == 0 else jnp.logical_not(low)
            one = jnp.where(mine, q, jnp.zeros_like(q))
            near = lax.dot_general(one, k, contract, preferred_element_type=jnp.float32)
            near = near * factor + table[h, min(block, 1)]
            far = lax.dot_general(one, ck, contract, preferred_element_type=jnp.float32)
            far = far * factor + far_ref[2 * pair + h] * LOG2E
            top = jnp.maximum(
                jnp.max(near, axis=-1, keepdims=True), jnp.max(far, axis=-1, keepdims=True)
            )
            near = jnp.exp2(near - top).astype(jnp.bfloat16)
            far = jnp.exp2(far - top).astype(jnp.bfloat16)
            got = jnp.dot(near, v, preferred_element_type=jnp.float32) + jnp.dot(
                far, cv, preferred_element_type=jnp.float32
            )
            halves.append(got[:, :lanes] / got[:, lanes:])
        outs.append(jnp.where(low, halves[0], halves[1]).reshape(rows_dev, WIN_COLS, lanes))
    outs = [outs[0][:, half:]] + outs[1:] + [outs[0][:, :half]]
    out_ref[0] = jnp.concatenate(outs, axis=1).astype(jnp.bfloat16)


def attention(query, pair, ctx_pair, rel_bias, ctx_bias):
    samples, rows_dev, _, cols = query.shape
    padded, ctx_count = pair.shape[1], ctx_pair.shape[0] * ctx_pair.shape[2]
    heads = cols // HEAD_DIM
    lanes = 2 * HEAD_DIM
    pairs = cols // lanes
    nq, nk = rows_dev * WIN_COLS, padded * 2 * WIN_COLS
    flat = jnp.pad(rel_bias, ((0, 0), (0, 1), (0, 1))).reshape(heads, -1)
    flat = jnp.pad(flat, ((0, 0), (0, nk - flat.shape[1]))).reshape(pairs, 2, nk)
    token = lambda at: pl.BlockSpec((1, padded, GRID_W, lanes), lambda p, s: (s, 0, 0, p + at))
    far = lambda at: pl.BlockSpec(
        (ctx_pair.shape[0], 1, ctx_pair.shape[2], lanes), lambda p, s: (0, s, 0, p + at)
    )
    own = pl.BlockSpec((1, rows_dev, GRID_W, lanes), lambda p, s: (s, 0, 0, p))
    scores = samples * heads * 4 * nq * (nk + ctx_count)
    return pl.pallas_call(
        attention_kernel,
        grid=(pairs, samples),
        out_shape=jax.ShapeDtypeStruct(query.shape, jnp.bfloat16),
        in_specs=[
            pl.BlockSpec((1, 2, nk), lambda p, s: (p, 0, 0)),
            pl.BlockSpec(memory_space=pltpu.SMEM),
            own,
            token(0),
            token(pairs),
            far(0),
            far(pairs),
        ],
        out_specs=own,
        scratch_shapes=[pltpu.VMEM((2, 2, nq, nk), jnp.float32)],
        cost_estimate=pl.CostEstimate(
            flops=scores * 512, bytes_accessed=8 * query.size * 2, transcendentals=scores
        ),
    )(flat, ctx_bias, query, pair, pair, ctx_pair, ctx_pair)


def on_device(
    latent,
    context,
    cond,
    ctx_cond,
    w_shift,
    w_scale,
    w_gate,
    norm_gain,
    w_query,
    w_key,
    w_value,
    w_out,
    rel_bias,
    ctx_bias,
):
    samples = latent.shape[0]
    rows_sp = w_shift.shape[0]
    local_cols = w_shift.shape[1]
    sp_index = lax.axis_index("sp")
    ada = silu_rows(jnp.concatenate([cond, ctx_cond[None, :]], axis=0))
    ada_rows = lax.dynamic_slice_in_dim(ada, sp_index * rows_sp, rows_sp, 1)
    partial_value = jnp.stack(
        [
            jnp.dot(ada_rows, weight, preferred_element_type=jnp.float32)
            for weight in (w_shift, w_scale, w_gate)
        ]
    )
    summed = lax.psum(partial_value, "sp")
    modulation = lax.all_gather(summed, "tp", axis=2, tiled=True)
    hidden = modulate_rows(
        latent, norm_gain, modulation[0, :samples, None, :], modulation[1, :samples, None, :]
    )
    w_triple = jnp.concatenate([w_query, w_key, w_value], axis=1)
    triple = jnp.dot(
        lax.all_gather(hidden, "tp", axis=1, tiled=True),
        w_triple,
        preferred_element_type=jnp.float32,
    ).astype(jnp.bfloat16)
    ctx_hidden = modulate_rows(context, norm_gain, modulation[0, samples], modulation[1, samples])
    w_pair = jnp.concatenate([w_key, w_value], axis=1)
    own_pair = jnp.dot(ctx_hidden, w_pair, preferred_element_type=jnp.float32).astype(jnp.bfloat16)
    ctx_pair = lax.all_gather(own_pair, "sp", axis=1, tiled=True)
    heads = local_cols // HEAD_DIM
    tokens_sp = triple.shape[1]
    rows_dev = tokens_sp // GRID_W
    rows_all = rows_dev * lax.axis_size("sp")
    reach = WIN_ROWS // 2
    query = triple[..., :local_cols].reshape(samples, rows_dev, GRID_W, local_cols)
    pair = triple[..., local_cols:].reshape(samples, rows_dev, GRID_W, 2 * local_cols)
    padded_pair = extended(pair, (("sp", 1),), reach)
    mixed = attention(query, padded_pair, ctx_pair[None], rel_bias, ctx_bias)
    attended = mixed.reshape(samples, tokens_sp, local_cols)
    attended = attended.transpose(1, 0, 2)
    update = lax.psum_scatter(
        jnp.einsum("tsc,cd->tsd", attended, w_out, preferred_element_type=jnp.float32).astype(
            jnp.bfloat16
        ),
        "tp",
        scatter_dimension=0,
        tiled=True,
    ).astype(jnp.float32)
    gate = modulation[2, :samples, None, :]
    result = latent.astype(jnp.float32) + gate * update.transpose(1, 0, 2)
    return result.astype(jnp.bfloat16)


MESH = pl.DeviceIdType.MESH


def entry_barrier(peers):
    barrier = pltpu.get_barrier_semaphore()
    for device, there in peers:
        @pl.when(there)
        def _():
            pl.semaphore_signal(barrier, inc=1, device_id=device, device_id_type=MESH)
    pl.semaphore_wait(barrier, sum(jnp.where(there, 1, 0) for _, there in peers))


def front_kernel(
    ada_ref, ws_ref, wc_ref, wg_ref, gain_ref, latent_ref, ctx_ref, wq_ref, wk_ref, wv_ref,
    full_ref, q_ref, kv_ref, ckv_ref,
    part, got, total, full, buf, wq, wkv, own_sem, s1, r1, s2, r2, s_ext, r_ext, s_ctx, r_ctx, r_sib,
):
    sp, tp = lax.axis_index("sp"), lax.axis_index("tp")
    n_sp, n_tp = lax.axis_size("sp"), lax.axis_size("tp")
    cols = part.shape[1]
    over_sp = [lax.rem(sp + k, n_sp) for k in range(1, n_sp)]
    over_tp = [lax.rem(tp + k, n_tp) for k in range(1, n_tp)]
    always = sp >= 0
    y, c = tp // 2, lax.rem(tp, 2)
    z, x = sp // 2, lax.rem(sp, 2)
    n_z = n_sp // 2
    sib, across = y * 2 + 1 - c, (1 - y) * 2 + c
    has_up, has_down = sp > 0, sp < n_sp - 1
    direct = y * c + (1 - y) * (6 + c)
    indirect = (1 - y) * c + y * (6 + c)
    has_direct = ((y == 1) & has_up) | ((y == 0) & has_down)
    has_indirect = ((y == 0) & has_up) | ((y == 1) & has_down)
    toward = sp + 2 * y - 1
    here, there = (sp, sib), (sp, across)
    own_slot, across_slot = 2 + tp, 2 + across
    x_peer = sp + 1 - 2 * x
    beside, up, down = (x_peer, tp), (sp + 2, tp), (sp - 2, tp)
    can_up, can_down = sp + 2 < n_sp, sp >= 2
    half = buf.shape[1] // 2
    part_of = pl.ds(pl.multiple_of(c * half, half), half)

    locals_ = [
        pltpu.make_async_copy(wq_ref, wq, own_sem.at[0]),
        pltpu.make_async_copy(wk_ref, wkv.at[:, pl.ds(0, cols)], own_sem.at[1]),
        pltpu.make_async_copy(wv_ref, wkv.at[:, pl.ds(cols, cols)], own_sem.at[2]),
    ]
    for copy in locals_:
        copy.start()
    own_copies = [
        pltpu.make_async_copy(latent_ref.at[s], buf.at[2 * own_slot + s], own_sem.at[3 + s])
        for s in range(2)
    ] + [
        pltpu.make_async_copy(ctx_ref.at[s], buf.at[16 + sp, pl.ds(half * s, half)], own_sem.at[5 + s])
        for s in range(2)
    ]
    for copy in own_copies:
        copy.start()
    entry_barrier([((p, tp), always) for p in over_sp] + [((sp, p), always) for p in over_tp])

    early = []
    mode = ["start"]

    def send(cond, copy):
        @pl.when(cond)
        def _():
            if mode[0] == "start":
                copy.start()
            else:
                copy.wait_send()

    def begin(cond, copy):
        early.append((cond, copy))
        send(cond, copy)

    def arrived(cond, copy):
        if mode[0] == "start":
            @pl.when(cond)
            def _():
                copy.wait_recv()

    def piece(flow, s, device, slot, own=False):
        return pltpu.make_async_remote_copy(
            src_ref=latent_ref.at[s] if own else buf.at[2 * slot + s],
            dst_ref=buf.at[2 * slot + s],
            send_sem=s_ext.at[flow, s], recv_sem=r_ext.at[flow, s],
            device_id=device, device_id_type=MESH,
        )

    def block(at, way, device, own=False):
        return pltpu.make_async_remote_copy(
            src_ref=ctx_ref.at[c] if own else buf.at[16 + at, part_of],
            dst_ref=buf.at[16 + at, part_of],
            send_sem=s_ctx.at[at, way], recv_sem=(r_sib if way == 3 else r_ctx).at[at],
            device_id=device, device_id_type=MESH,
        )

    def first(k, peer):
        return pltpu.make_async_remote_copy(
            src_ref=part, dst_ref=got.at[k], send_sem=s1.at[k], recv_sem=r1.at[k],
            device_id=(peer, tp), device_id_type=MESH,
        )

    columns = pl.ds(pl.multiple_of(tp * cols, cols), cols)

    def second(k, peer):
        return pltpu.make_async_remote_copy(
            src_ref=total, dst_ref=full.at[:, columns], send_sem=s2.at[k], recv_sem=r2.at[k],
            device_id=(sp, peer), device_id_type=MESH,
        )

    for at, weight in enumerate((ws_ref, wc_ref, wg_ref)):
        value = jnp.dot(ada_ref[...], weight[...], preferred_element_type=jnp.float32)
        part[8 * at : 8 * at + 8, :] = value[:8]
    firsts = [first(k, peer) for k, peer in enumerate(over_sp)]
    for copy in firsts:
        copy.start()
    begin(always, piece(1, 0, there, own_slot, True))
    begin(always, block(sp, 0, beside, True))
    begin(can_up, block(sp, 1, up, True))
    begin(can_down, block(sp, 2, down, True))
    for s in range(2):
        begin(has_indirect, piece(2, s, (toward, tp), direct, True))
    for s in range(2):
        begin(always, piece(0, s, here, own_slot, True))
    value = part[...]
    for k, copy in enumerate(firsts):
        copy.wait()
        value = value + got[k]
    total[...] = value
    seconds = [second(k, peer) for k, peer in enumerate(over_tp)]
    for copy in seconds:
        copy.start()
    begin(always, piece(1, 1, there, own_slot, True))
    full[:, columns] = value
    for copy in locals_ + own_copies:
        copy.wait()
    for copy in seconds:
        copy.wait()
    full_ref[...] = full[...]

    def neighbour_block():
        arrived(always, block(x_peer, 0, beside))
        send((c == 0) & can_up, block(x_peer, 1, up))
        send((c == 0) & can_down, block(x_peer, 2, down))
        send(always, block(x_peer, 3, here))

    def relay(hop):
        for e in range(2):
            straight = (c == 0) | (x == e)
            crossing = (c == 1) & (x == e)
            low, high = sp - x - 2 * hop + e, sp - x + 2 * hop + e
            for at, way, device, can, there_is in (
                (lax.max(low, 0), 1, up, can_up, low >= 0),
                (lax.min(high, n_sp - 1), 2, down, can_down, high < n_sp),
            ):
                arrived(there_is, block(at, way, device))
                send(there_is & can & straight, block(at, way, device))
                send(there_is & crossing, block(at, 0, beside))
                send(there_is, block(at, 3, here))

    def from_across(s):
        arrived(always, piece(1, s, there, across_slot))
        send(always, piece(3, s, here, across_slot))

    def from_direct(s):
        arrived(has_direct, piece(2, s, here, direct))
        send(has_direct, piece(5, s, there, direct))
        send(has_direct, piece(6, s, here, direct))

    def from_indirect(s):
        arrived(has_indirect, piece(5, s, there, indirect))
        send(has_indirect, piece(7, s, here, indirect))

    def sibling(flow, s, cond=always):
        arrived(cond, piece(flow, s, here, own_slot))

    def far_block(h, e):
        zb = lax.rem(z + h, n_z)
        at = 2 * zb + e
        arrived(always, block(at, 3, here))

    plan = []

    def add(kind, s, events, at=0):
        plan.append((kind, s, events, at))

    both = lambda flow, cond=always: [functools.partial(sibling, flow, e, cond) for e in range(2)]
    add(0, 0, [])
    add(1, 0, [neighbour_block] + both(0))
    from_peer = lambda: arrived(always, block(x_peer, 3, here))
    add(8, 0, [functools.partial(from_across, 0), functools.partial(from_direct, 0), from_peer], 2 * z)
    add(2, 0, [functools.partial(relay, 1), functools.partial(from_across, 1)])
    add(4, 0, [functools.partial(from_direct, 1)])
    add(3, 0, [functools.partial(relay, 2)] + both(3))
    add(5, 0, both(6, has_direct))
    hops = [functools.partial(relay, hop) for hop in range(3, n_z)]
    for h in range(1, n_z):
        waits = [functools.partial(far_block, h, e) for e in range(2)]
        add(8, 0, (hops + [functools.partial(from_indirect, 0)] if h == 1 else []) + waits, 2 * lax.rem(z + h, n_z))
    add(6, 0, [functools.partial(from_indirect, 1)])
    add(7, 0, both(7, has_indirect))

    slots = (own_slot, 2 + sib, across_slot, 2 + (1 - y) * 2 + 1 - c,
             direct, direct + 1 - 2 * c, indirect, indirect + 1 - 2 * c)

    def step(i, carry):
        at = 0
        row = 0
        exists = 0
        wants = 0
        for k, (kind, s, events, ctx_at) in enumerate(plan):
            on = jnp.where(i == k, 1, 0)
            at = at + on * (16 + ctx_at if kind == 8 else 2 * slots[kind])
            row = row + on * (1 if kind == 8 else 0)
            there_is = has_direct if kind in (4, 5) else has_indirect if kind in (6, 7) else always
            exists = exists + on * jnp.where(there_is, 1, 0)
            wants = wants + on * (1 if kind < 4 else 0)
            if events:
                @pl.when(i == k)
                def _():
                    for event in events:
                        event()

        @pl.when(exists == 1)
        def _():
            hidden = []
            for e in range(2):
                rows = buf[at + e].astype(jnp.float32)
                inverse = lax.rsqrt(jnp.mean(rows * rows, axis=-1, keepdims=True) + EPSILON)
                which = e + row * (2 - e)
                lift = gain_ref[...] * (1.0 + full[pl.ds(8 + which, 1), :])
                rows = rows * inverse * lift + full[pl.ds(which, 1), :]
                hidden.append(rows.astype(jnp.bfloat16))
            hidden = jnp.concatenate(hidden, axis=0)
            count = hidden.shape[0] // 2
            pair = jnp.dot(hidden, wkv[...], preferred_element_type=jnp.float32).astype(jnp.bfloat16)

            @pl.when(at < 16)
            def _():
                for e in range(2):
                    kv_ref[lax.div(lax.min(at, 14), 2) + 8 * e] = pair[e * count : (e + 1) * count]

            @pl.when(at >= 16)
            def _():
                for e in range(2):
                    ckv_ref[lax.max(at - 16, 0) + e] = pair[e * count : (e + 1) * count]

            @pl.when(wants == 1)
            def _():
                query = jnp.dot(hidden, wq[...], preferred_element_type=jnp.float32)
                query = query.astype(jnp.bfloat16)
                for e in range(2):
                    place = lax.div(lax.min(lax.max(at - 4, 0), 6), 2) + 4 * e
                    q_ref[place] = query[e * count : (e + 1) * count]

        @pl.when(exists == 0)
        def _():
            for e in range(2):
                kv_ref[lax.div(lax.min(at, 14), 2) + 8 * e] = jnp.zeros(kv_ref.shape[1:], jnp.bfloat16)

        return carry

    lax.fori_loop(0, len(plan), step, 0)
    mode[0] = "drain"
    for cond, copy in early:
        send(cond, copy)
    for _, _, events, _ in plan:
        for event in events:
            event()


def front(ada_rows, mods, gain, latent, context, w_query, w_key, w_value):
    n_sp, n_tp = lax.axis_size("sp"), lax.axis_size("tp")
    samples, tokens, width = latent.shape
    cols = w_query.shape[1]
    block = (24, cols)
    ada_rows = jnp.pad(ada_rows, ((0, 16 - ada_rows.shape[0]), (0, 0)))
    vmem, hbm = pl.BlockSpec(memory_space=pltpu.VMEM), pl.BlockSpec(memory_space=pl.ANY)
    dma = pltpu.SemaphoreType.DMA
    return pl.pallas_call(
        front_kernel,
        out_shape=(
            jax.ShapeDtypeStruct((24, width), jnp.float32),
            jax.ShapeDtypeStruct((samples * n_tp, tokens, cols), jnp.bfloat16),
            jax.ShapeDtypeStruct((samples * 8, tokens, 2 * cols), jnp.bfloat16),
            jax.ShapeDtypeStruct((n_sp, samples * context.shape[1], 2 * cols), jnp.bfloat16),
        ),
        in_specs=[vmem] * 7 + [hbm] * 3,
        out_specs=[vmem] * 4,
        scratch_shapes=[
            pltpu.VMEM(block, jnp.float32),
            pltpu.VMEM((n_sp - 1,) + block, jnp.float32),
            pltpu.VMEM(block, jnp.float32),
            pltpu.VMEM((24, width), jnp.float32),
            pltpu.VMEM((16 + n_sp, tokens, width), jnp.bfloat16),
            pltpu.VMEM((width, cols), jnp.bfloat16),
            pltpu.VMEM((width, 2 * cols), jnp.bfloat16),
            dma((7,)), dma((n_sp - 1,)), dma((n_sp - 1,)), dma((n_tp - 1,)), dma((n_tp - 1,)),
            dma((8, 2)), dma((8, 2)), dma((n_sp, 4)), dma((n_sp,)), dma((n_sp,)),
        ],
        compiler_params=pltpu.CompilerParams(
            collective_id=1, has_side_effects=True, vmem_limit_bytes=60 * 2**20
        ),
    )(ada_rows, *mods, gain[None, :], latent, context, w_query, w_key, w_value)


def scatter_kernel(parts_ref, out_ref, got, summed, far, s1, r1, s2, r2):
    sp, tp = lax.axis_index("sp"), lax.axis_index("tp")
    y, c = tp // 2, lax.rem(tp, 2)
    sib, across = y * 2 + 1 - c, (1 - y) * 2 + c
    sib_across = (1 - y) * 2 + 1 - c
    entry_barrier([((sp, sib), sp >= 0), ((sp, across), sp >= 0)])
    chunks = far.shape[0]
    rows = far.shape[1]

    def near(k):
        at = k % chunks
        target = sib_across if k < chunks else sib
        return pltpu.make_async_remote_copy(
            src_ref=parts_ref.at[target, pl.ds(at * rows, rows)],
            dst_ref=got.at[k],
            send_sem=s1.at[k], recv_sem=r1.at[k],
            device_id=(sp, sib), device_id_type=MESH,
        )

    def cross(k):
        return pltpu.make_async_remote_copy(
            src_ref=summed.at[k],
            dst_ref=far.at[k],
            send_sem=s2.at[k], recv_sem=r2.at[k],
            device_id=(sp, across), device_id_type=MESH,
        )

    for k in range(2 * chunks):
        near(k).start()
    for k in range(chunks):
        near(k).wait()
        mine = parts_ref[across, k * rows : (k + 1) * rows, :].astype(jnp.float32)
        summed[k] = (mine + got[k].astype(jnp.float32)).astype(jnp.bfloat16)
        cross(k).start()
    for k in range(chunks):
        near(chunks + k).wait()
        cross(k).wait()
        mine = parts_ref[tp, k * rows : (k + 1) * rows, :].astype(jnp.float32)
        mine = mine + got[chunks + k].astype(jnp.float32) + far[k].astype(jnp.float32)
        out_ref[k * rows : (k + 1) * rows, :] = mine


def scatter_sum(parts):
    _, tokens, width = parts.shape
    chunks = 4
    rows = tokens // chunks
    sems = [pltpu.SemaphoreType.DMA((2 * chunks,))] * 2 + [pltpu.SemaphoreType.DMA((chunks,))] * 2
    return pl.pallas_call(
        scatter_kernel,
        out_shape=jax.ShapeDtypeStruct((tokens, width), jnp.float32),
        in_specs=[pl.BlockSpec(memory_space=pltpu.VMEM)],
        out_specs=pl.BlockSpec(memory_space=pltpu.VMEM),
        scratch_shapes=[
            pltpu.VMEM((2 * chunks, rows, width), jnp.bfloat16),
            pltpu.VMEM((chunks, rows, width), jnp.bfloat16),
            pltpu.VMEM((chunks, rows, width), jnp.bfloat16),
        ]
        + sems,
        compiler_params=pltpu.CompilerParams(
            collective_id=3, has_side_effects=True, vmem_limit_bytes=40 * 2**20
        ),
    )(parts)


def on_four(
    latent, context, cond, ctx_cond, w_shift, w_scale, w_gate, norm_gain,
    w_query, w_key, w_value, w_out, rel_bias, ctx_bias,
):
    samples, tokens, width = latent.shape
    n_sp, n_tp = lax.axis_size("sp"), lax.axis_size("tp")
    rows_sp, local_cols = w_shift.shape
    sp = lax.axis_index("sp")
    ada = silu_rows(jnp.concatenate([cond, ctx_cond[None, :]], axis=0))
    ada_rows = lax.dynamic_slice_in_dim(ada, sp * rows_sp, rows_sp, 1)
    modulation, query, pair, ctx_pair = front(
        ada_rows, (w_shift, w_scale, w_gate), norm_gain, latent, context, w_query, w_key, w_value
    )
    modulation = modulation.reshape(3, 8, width)
    rows_dev = n_tp * tokens // GRID_W
    query = query.reshape(samples, rows_dev, GRID_W, local_cols)
    pair = pair.reshape(samples, 2 * rows_dev, GRID_W, 2 * local_cols)
    ctx_pair = ctx_pair.reshape(n_sp, samples, -1, 2 * local_cols)
    mixed = attention(query, pair, ctx_pair, rel_bias, ctx_bias)
    attended = mixed.reshape(samples, n_tp, tokens, local_cols)
    attended = attended.transpose(1, 0, 2, 3).reshape(n_tp, samples * tokens, local_cols)
    parts = jnp.dot(attended, w_out, preferred_element_type=jnp.float32).astype(jnp.bfloat16)
    update = scatter_sum(parts).reshape(samples, tokens, width)
    gate = modulation[2, :samples, None, :]
    return (latent.astype(jnp.float32) + gate * update).astype(jnp.bfloat16)


def solution(mesh):
    shape = dict(mesh.shape)
    quick = shape["tp"] == 4 and shape["sp"] == 8
    return jax.shard_map(
        on_four if quick else on_device,
        mesh=mesh,
        in_specs=(
            P(None, ("sp", "tp"), None),
            P(None, "sp", None),
            P(),
            P(),
            P("sp", "tp"),
            P("sp", "tp"),
            P("sp", "tp"),
            P(),
            P(None, "tp"),
            P(None, "tp"),
            P(None, "tp"),
            P("tp", None),
            P("tp", None, None),
            P("tp"),
        ),
        out_specs=P(None, ("sp", "tp"), None),
        check_vma=False,
    )
```

profile of v0, /device:TPU:0, one launch (start us, length us, event | category | flops | bytes accessed | tf_op | source)
XLA Modules:
  0.0 139.8 jit_solution(16422913198282073390)
XLA Ops:
  0.0 0.0 copy-start
  0.0 0.8 broadcast_in_dim.6
  0.8 0.7 maximum_convert_fusion
  1.6 0.6 pad.8.ada_ref
  2.2 0.8 copy.17
  3.1 0.7 reshape.28.bias_ref
  3.8 84.8 %shard_map.136 = (f32[24,2048]{1,0:T(8,128)}, bf16[8,128,512]{2,1,0:T(8,128)(2,1)}, bf16[16,128,1024]{2,1,0:T(8,128)(2,1)}, bf16[8,128,1024]{2,1,0:T(8,128)(2,1)}) custom-call(bf16[16,256]{1,0:T(8,128)(2,1)} %pad.8.ada_ref, bf16[256,512]{1,0:T(8,128)(2,1)} %ws_ref.1, bf16[256,512]{1,0:T(8,128)(2,1)} %wc_ref.1, bf16[256,512]{1,0:T(8,128)(2,1)} %wg_ref.1, ...), custom_call_target="tpu_custom_call" | custom-call | tf_op jit(solution)/shard_map/pallas_call | solution.py:505
  88.5 0.8 slice_bitcast_fusion
  89.4 16.4 %shard_map.137 = bf16[2,8,64,512]{3,2,1,0:T(8,128)(2,1)} custom-call(f32[4,2,512]{2,1,0:T(2,128)} %reshape.28.bias_ref, f32[8]{0:T(128)} %far_ref.1, bf16[2,8,64,512]{3,2,1,0:T(8,128)(2,1)} %bitcast.25, bf16[2,16,64,1024]{3,2,1,0:T(8,128)(2,1)} %bitcast.21, bf16[2,16,64,1024]{3,2,1,0:T(8,128)(2,1)} %bitcast.22, bf16[8,2,64,1024]{3,2,1,0:T(8,128)(2,1)} %bitcast.23, ...), custom_call_target="tpu_custom_call" | custom-call | flops 4294967296 | bytes 8388608 | tf_op jit(solution)/shard_map/pallas_call | solution.py:138
  105.8 1.3 copy.16
  107.1 0.0 copy-done
  107.1 2.3 %convolution_convert_fusion.parts_ref = bf16[4,256,2048]{2,1,0:T(8,128)(2,1)S(1)} fusion(bf16[4,256,512]{2,1,0:T(8,128)(2,1)S(1)} %bitcast.18, bf16[512,2048]{1,0:T(8,128)(2,1)S(1)} %copy-done), kind=kOutput, calls=%fused_computation | convolution fusion | flops 2149580800 | bytes 7340032 | tf_op jit(solution)/shard_map/dot_general | solution.py:617
  109.5 0.0 copy-start.1
  109.5 29.0 %shard_map.138 = f32[256,2048]{1,0:T(8,128)S(1)} custom-call(bf16[4,256,2048]{2,1,0:T(8,128)(2,1)S(1)} %convolution_convert_fusion.parts_ref), custom_call_target="tpu_custom_call" | custom-call | tf_op jit(solution)/shard_map/pallas_call | solution.py:579
  138.5 0.0 copy-done.1
  138.5 1.3 add_convert_fusion
  (2 shorter events, 0.0 us)
Async XLA Ops:
  0.0 107.1 %copy-start = (bf16[512,2048]{1,0:T(8,128)(2,1)S(1)}, bf16[512,2048]{1,0:T(8,128)(2,1)}, u32[]{:S(2)}) copy-start(bf16[512,2048]{1,0:T(8,128)(2,1)} %param.25) | copy-start | bytes 6291460
  109.5 29.0 %copy-start.1 = (bf16[2,128,2048]{2,1,0:T(8,128)(2,1)S(1)}, bf16[2,128,2048]{2,1,0:T(8,128)(2,1)}, u32[]{:S(2)}) copy-start(bf16[2,128,2048]{2,1,0:T(8,128)(2,1)} %latent_ref.1) | copy-start | bytes 3145732
where the time goes:
time: 140 us
  Pallas kernels  130 us (93%)
  local copies, waits for them, and re-layouts  5.18 us (4%)
  matrix products  2.34 us (2%)
  other arithmetic  2.01 us (1%)
    pallas_call x1, Pallas kernels, front(): pl.pallas_call(front_kernel, out_shape=(jax.ShapeDtypeStruct((24, width),...  84.8 us
    pallas_call x1, Pallas kernels, scatter_sum(): pl.pallas_call(scatter_kernel, out_shape=jax.ShapeDtypeStruct((tokens, wi...  29 us
    pallas_call x1, Pallas kernels, attention(): pl.pallas_call(attention_kernel, grid=(pairs, samples), out_shape=jax.Sha...  16.4 us

commit v1 on v0

v1 whole, which is shorter than its diff:
```python
import functools

import jax
import jax.numpy as jnp
from jax import lax
from jax.experimental import pallas as pl
from jax.experimental.pallas import tpu as pltpu
from jax.sharding import PartitionSpec as P

HEAD_DIM = 64
GRID_W = 64
WIN_ROWS = 8
WIN_COLS = 16


EPSILON = 1e-06


def extended(shard, sides, width):
    for axis, dim in sides:
        size, length = (lax.axis_size(axis), shard.shape[dim])
        up = [(i, (i + 1) % size) for i in range(size - 1)]
        down = [(j, i) for i, j in up]
        last = lax.slice_in_dim(shard, length - width, length, axis=dim)
        first = lax.slice_in_dim(shard, 0, width, axis=dim)
        before = lax.ppermute(last, axis, up)
        after = lax.ppermute(first, axis, down)
        shard = jnp.concatenate([before, shard, after], axis=dim)
    return shard


def silu_rows(values):
    return jax.nn.silu(values.astype(jnp.float32)).astype(jnp.bfloat16)


def modulate_rows(rows, gain, shift, scale):
    floats = rows.astype(jnp.float32)
    inverse = lax.rsqrt(jnp.mean(floats * floats, axis=-1, keepdims=True) + EPSILON)
    return (floats * inverse * gain * (1.0 + scale) + shift).astype(jnp.bfloat16)

LOG2E = 1.4426950408889634


def attention_kernel(bias_ref, far_ref, q_ref, k_ref, v_ref, ck_ref, cv_ref, out_ref, table):
    pair = pl.program_id(0)
    rows_dev = q_ref.shape[1]
    padded = k_ref.shape[1]
    span = 2 * WIN_COLS
    half = WIN_COLS // 2
    reach = WIN_ROWS // 2
    nq, nk = rows_dev * WIN_COLS, padded * span
    lanes = 2 * HEAD_DIM

    @pl.when(pl.program_id(1) == 0)
    def _():
        sp = lax.axis_index("sp")
        rows_all = rows_dev * lax.axis_size("sp")
        at = lax.broadcasted_iota(jnp.int32, (WIN_COLS, nk), 1)
        p = lax.broadcasted_iota(jnp.int32, (WIN_COLS, nk), 0)
        key_row = sp * rows_dev - reach + at // span
        k = at % span
        inner = (k - p >= 0) & (k - p < WIN_COLS)
        edge = (p < half) == (k < WIN_COLS)
        for r in range(rows_dev):
            row = sp * rows_dev + r
            first = jnp.clip(row - reach, 0, rows_all - WIN_ROWS)
            inside = (key_row >= first) & (key_row < first + WIN_ROWS)
            shift = span * (r + reach - WIN_ROWS + 1) - half + 1
            for h in range(2):
                line = jnp.broadcast_to(bias_ref[0, h : h + 1, :], (WIN_COLS, nk))
                line = pltpu.roll(line, shift % nk, 1, stride=1, stride_axis=0) * LOG2E
                at_rows = pl.ds(r * WIN_COLS, WIN_COLS)
                table[h, 0, at_rows, :] = jnp.where(inside & edge, line, -jnp.inf)
                table[h, 1, at_rows, :] = jnp.where(inside & inner, line, -jnp.inf)

    factor = HEAD_DIM ** (-0.5) * LOG2E
    ck = ck_ref[...].reshape(-1, lanes)
    ctx_count = ck.shape[0]
    cv = jnp.concatenate([cv_ref[...].reshape(-1, lanes), jnp.ones((ctx_count, lanes), jnp.bfloat16)], axis=1)
    ones = jnp.ones((nk, lanes), jnp.bfloat16)
    low = lax.broadcasted_iota(jnp.int32, (nq, lanes), 1) < HEAD_DIM
    contract = (((1,), (1,)), ((), ()))
    every = q_ref[0].astype(jnp.float32)
    outs = []
    for block in range(GRID_W // WIN_COLS):
        if block == 0:
            q = jnp.concatenate([every[:, GRID_W - half :], every[:, :half]], axis=1)
        else:
            q = every[:, WIN_COLS * block - half : WIN_COLS * (block + 1) - half]
        q = q.astype(jnp.bfloat16).reshape(nq, lanes)

        def keys(ref):
            if block == 0:
                got = jnp.concatenate([ref[0, :, GRID_W - WIN_COLS :, :], ref[0, :, :WIN_COLS, :]], 1)
            else:
                got = ref[0, :, WIN_COLS * (block - 1) : WIN_COLS * (block + 1), :]
            return got.reshape(nk, lanes)

        k = keys(k_ref)
        v = jnp.concatenate([keys(v_ref), ones], axis=1)
        halves = []
        for h in range(2):
            mine = low if h == 0 else jnp.logical_not(low)
            one = jnp.where(mine, q, jnp.zeros_like(q))
            near = lax.dot_general(one, k, contract, preferred_element_type=jnp.float32)
            near = near * factor + table[h, min(block, 1)]
            far = lax.dot_general(one, ck, contract, preferred_element_type=jnp.float32)
            far = far * factor + far_ref[2 * pair + h] * LOG2E
            top = jnp.maximum(
                jnp.max(near, axis=-1, keepdims=True), jnp.max(far, axis=-1, keepdims=True)
            )
            near = jnp.exp2(near - top).astype(jnp.bfloat16)
            far = jnp.exp2(far - top).astype(jnp.bfloat16)
            got = jnp.dot(near, v, preferred_element_type=jnp.float32) + jnp.dot(
                far, cv, preferred_element_type=jnp.float32
            )
            halves.append(got[:, :lanes] / got[:, lanes:])
        outs.append(jnp.where(low, halves[0], halves[1]).reshape(rows_dev, WIN_COLS, lanes))
    outs = [outs[0][:, half:]] + outs[1:] + [outs[0][:, :half]]
    out_ref[0] = jnp.concatenate(outs, axis=1).astype(jnp.bfloat16)


def attention(query, pair, ctx_pair, rel_bias, ctx_bias):
    samples, rows_dev, _, cols = query.shape
    padded, ctx_count = pair.shape[1], ctx_pair.shape[0] * ctx_pair.shape[2]
    heads = cols // HEAD_DIM
    lanes = 2 * HEAD_DIM
    pairs = cols // lanes
    nq, nk = rows_dev * WIN_COLS, padded * 2 * WIN_COLS
    flat = jnp.pad(rel_bias, ((0, 0), (0, 1), (0, 1))).reshape(heads, -1)
    flat = jnp.pad(flat, ((0, 0), (0, nk - flat.shape[1]))).reshape(pairs, 2, nk)
    token = lambda at: pl.BlockSpec((1, padded, GRID_W, lanes), lambda p, s: (s, 0, 0, p + at))
    far = lambda at: pl.BlockSpec(
        (ctx_pair.shape[0], 1, ctx_pair.shape[2], lanes), lambda p, s: (0, s, 0, p + at)
    )
    own = pl.BlockSpec((1, rows_dev, GRID_W, lanes), lambda p, s: (s, 0, 0, p))
    scores = samples * heads * 4 * nq * (nk + ctx_count)
    return pl.pallas_call(
        attention_kernel,
        grid=(pairs, samples),
        out_shape=jax.ShapeDtypeStruct(query.shape, jnp.bfloat16),
        in_specs=[
            pl.BlockSpec((1, 2, nk), lambda p, s: (p, 0, 0)),
            pl.BlockSpec(memory_space=pltpu.SMEM),
            own,
            token(0),
            token(pairs),
            far(0),
            far(pairs),
        ],
        out_specs=own,
        scratch_shapes=[pltpu.VMEM((2, 2, nq, nk), jnp.float32)],
        cost_estimate=pl.CostEstimate(
            flops=scores * 512, bytes_accessed=8 * query.size * 2, transcendentals=scores
        ),
    )(flat, ctx_bias, query, pair, pair, ctx_pair, ctx_pair)


def on_device(
    latent,
    context,
    cond,
    ctx_cond,
    w_shift,
    w_scale,
    w_gate,
    norm_gain,
    w_query,
    w_key,
    w_value,
    w_out,
    rel_bias,
    ctx_bias,
):
    samples = latent.shape[0]
    rows_sp = w_shift.shape[0]
    local_cols = w_shift.shape[1]
    sp_index = lax.axis_index("sp")
    ada = silu_rows(jnp.concatenate([cond, ctx_cond[None, :]], axis=0))
    ada_rows = lax.dynamic_slice_in_dim(ada, sp_index * rows_sp, rows_sp, 1)
    partial_value = jnp.stack(
        [
            jnp.dot(ada_rows, weight, preferred_element_type=jnp.float32)
            for weight in (w_shift, w_scale, w_gate)
        ]
    )
    summed = lax.psum(partial_value, "sp")
    modulation = lax.all_gather(summed, "tp", axis=2, tiled=True)
    hidden = modulate_rows(
        latent, norm_gain, modulation[0, :samples, None, :], modulation[1, :samples, None, :]
    )
    w_triple = jnp.concatenate([w_query, w_key, w_value], axis=1)
    triple = jnp.dot(
        lax.all_gather(hidden, "tp", axis=1, tiled=True),
        w_triple,
        preferred_element_type=jnp.float32,
    ).astype(jnp.bfloat16)
    ctx_hidden = modulate_rows(context, norm_gain, modulation[0, samples], modulation[1, samples])
    w_pair = jnp.concatenate([w_key, w_value], axis=1)
    own_pair = jnp.dot(ctx_hidden, w_pair, preferred_element_type=jnp.float32).astype(jnp.bfloat16)
    ctx_pair = lax.all_gather(own_pair, "sp", axis=1, tiled=True)
    heads = local_cols // HEAD_DIM
    tokens_sp = triple.shape[1]
    rows_dev = tokens_sp // GRID_W
    rows_all = rows_dev * lax.axis_size("sp")
    reach = WIN_ROWS // 2
    query = triple[..., :local_cols].reshape(samples, rows_dev, GRID_W, local_cols)
    pair = triple[..., local_cols:].reshape(samples, rows_dev, GRID_W, 2 * local_cols)
    padded_pair = extended(pair, (("sp", 1),), reach)
    mixed = attention(query, padded_pair, ctx_pair[None], rel_bias, ctx_bias)
    attended = mixed.reshape(samples, tokens_sp, local_cols)
    attended = attended.transpose(1, 0, 2)
    update = lax.psum_scatter(
        jnp.einsum("tsc,cd->tsd", attended, w_out, preferred_element_type=jnp.float32).astype(
            jnp.bfloat16
        ),
        "tp",
        scatter_dimension=0,
        tiled=True,
    ).astype(jnp.float32)
    gate = modulation[2, :samples, None, :]
    result = latent.astype(jnp.float32) + gate * update.transpose(1, 0, 2)
    return result.astype(jnp.bfloat16)


MESH = pl.DeviceIdType.MESH


def entry_barrier(peers):
    barrier = pltpu.get_barrier_semaphore()
    for device in peers:
        pl.semaphore_signal(barrier, inc=1, device_id=device, device_id_type=MESH)
    pl.semaphore_wait(barrier, len(peers))


def block_kernel(
    far_ref, flat_ref, gain_ref, cond_ref, ctx_cond_ref,
    ws_ref, wc_ref, wg_ref, latent_ref, ctx_ref, wq_ref, wk_ref, wv_ref, wo_ref,
    out_ref,
    ada, wm, part, got, total, full, buf, other, cx, cs, wq, wkv, wo, kv, qs, ckv, table,
    att, att_in, parts, y_in, fwd, x_in,
    own_sem, s1, r1, s2, r2, s_c, r_c, s_x, r_x, s_y, r_y, s_d, r_d, s_z, r_z, s_h, r_h,
    s_w, r_w, s_a, r_a, s_p, r_p, s_f, r_f,
):
    sp, tp = lax.axis_index("sp"), lax.axis_index("tp")
    n_sp, n_tp = lax.axis_size("sp"), lax.axis_size("tp")
    y, c = tp // 2, lax.rem(tp, 2)
    z, x = sp // 2, lax.rem(sp, 2)
    n_z = n_sp // 2
    same = x == y
    differs = x != y
    tokens, width = other.shape
    cols = wq.shape[1]
    rows_mod = wm.shape[1]
    lanes = 2 * HEAD_DIM
    pairs = cols // lanes
    half = WIN_COLS // 2
    reach = WIN_ROWS // 2
    own_rows = tokens // GRID_W
    group_rows = 2 * own_rows
    layer_rows = 4 * group_rows
    chunks = s_x.shape[0]
    size = tokens // chunks
    over_sp = [lax.rem(sp + k, n_sp) for k in range(1, n_sp)]
    over_tp = [lax.rem(tp + k, n_tp) for k in range(1, n_tp)]
    sib, across = (sp, tp + 1 - 2 * c), (sp, (1 - y) * 2 + c)
    beside = (sp + 1 - 2 * x, tp)
    g_own, g_x, g_y, g_d = 2 * x + y, 2 * (1 - x) + y, 2 * x + 1 - y, 2 * (1 - x) + 1 - y
    drain = []

    def remote(src, dst, s, r, device):
        return pltpu.make_async_remote_copy(
            src_ref=src, dst_ref=dst, send_sem=s, recv_sem=r, device_id=device, device_id_type=MESH
        )

    def begin(make, cond=None):
        drain.append((make, cond))
        if cond is None:
            make().start()
        else:
            @pl.when(cond)
            def _():
                make().start()

    def local(k, src, dst):
        copy = pltpu.make_async_copy(src, dst, own_sem.at[k])
        copy.start()
        return copy

    mod_copies = [local(k, w, wm.at[k]) for k, w in enumerate((ws_ref, wc_ref, wg_ref))]
    other_copy = local(3, latent_ref.at[1 - x], other)
    own_copy = local(4, latent_ref.at[x], buf.at[2 * g_own + c])
    ctx_half = cs.shape[0]
    ctx_part = lambda k: pl.ds(pl.multiple_of(k * ctx_half, ctx_half), ctx_half)
    stage_copy = local(5, ctx_ref.at[1 - x, ctx_part(c)], cs)
    ctx_copy = local(6, ctx_ref.at[x], cx.at[x])
    weight_copies = [
        local(7, wk_ref, wkv.at[:, pl.ds(0, cols)]),
        local(8, wv_ref, wkv.at[:, pl.ds(cols, cols)]),
        local(9, wq_ref, wq),
        local(10, wo_ref, wo.at[0]),
    ]
    entry_barrier([(p, tp) for p in over_sp] + [(sp, p) for p in over_tp])

    def piece(g, h):
        return buf.at[2 * g + c, pl.ds(h * size, size)]

    def to_beside(h):
        return remote(other.at[pl.ds(h * size, size)], piece(g_own, h), s_x.at[h], r_x.at[h], beside)

    def from_beside(h):
        return remote(other.at[pl.ds(h * size, size)], piece(g_x, h), s_x.at[h], r_x.at[h], beside)

    def over_y(g, flow, h):
        return remote(piece(g, h), piece(g, h), s_y.at[flow, h], r_y.at[flow, h], across)

    def to_sib(k, g, h):
        return remote(piece(g, h), piece(g, h), s_d.at[k, h], r_d.at[k, h], sib)

    def from_sib(k, g, h):
        there = buf.at[2 * g + 1 - c, pl.ds(h * size, size)]
        return remote(there, there, s_d.at[k, h], r_d.at[k, h], sib)

    mine = pl.ds(pl.multiple_of(sp * rows_mod, rows_mod), rows_mod)
    ada[...] = jnp.zeros_like(ada)
    ada[0:2, :] = cond_ref[:, mine].astype(jnp.float32)
    ada[2:3, :] = ctx_cond_ref[:, mine].astype(jnp.float32)
    values = ada[...]
    values = (values / (1.0 + jnp.exp(-values))).astype(jnp.bfloat16)
    at = 0
    for k, count in enumerate((3, 3, 2)):
        mod_copies[k].wait()
        value = jnp.dot(values, wm[k], preferred_element_type=jnp.float32)
        part[at : at + count, :] = value[:count]
        at += count
    for k, peer in enumerate(over_sp):
        begin(functools.partial(remote, part, got.at[k], s1.at[k], r1.at[k], (peer, tp)))

    stage_copy.wait()
    begin(lambda: remote(cs, cx.at[x, ctx_part(c)], s_c.at[0], r_c.at[0], beside))
    other_copy.wait()
    own_copy.wait()
    for h in range(chunks):
        if h < 2:
            begin(functools.partial(over_y, g_own, 0, h))
        begin(functools.partial(to_beside, h))
    for h in range(chunks):
        begin(functools.partial(to_sib, 0, g_own, h))

    span = 2 * WIN_COLS
    nk = table.shape[-1]
    nq = table.shape[-2] // 2
    rows_all = layer_rows * n_z
    lane = lax.broadcasted_iota(jnp.int32, (WIN_COLS, nk), 1)
    p = lax.broadcasted_iota(jnp.int32, (WIN_COLS, nk), 0)
    k_row, k_col = lane // span, lane % span
    inner = (k_col - p >= 0) & (k_col - p < WIN_COLS)
    edge = (p < half) == (k_col < WIN_COLS)

    def tables(pair, carry):
        for h in range(2):
            line = flat_ref[pl.ds(2 * pair + h, 1), :]
            line = jnp.broadcast_to(line, (WIN_COLS, line.shape[1]))
            for r in range(group_rows):
                shift = (span * (r + reach - WIN_ROWS + 1) - half + 1) % line.shape[1]
                rolled = pltpu.roll(line, shift, 1, stride=1, stride_axis=0)[:, :nk] * LOG2E
                at_rows = pl.ds(h * nq + r * WIN_COLS, WIN_COLS)
                for kind in range(3):
                    row = z * layer_rows + r + (0, 0, layer_rows - group_rows)[kind]
                    first = row - reach
                    if kind:
                        first = jnp.clip(first, 0, rows_all - WIN_ROWS)
                    key_row = k_row + (row - r - reach)
                    inside = (key_row >= first) & (key_row < first + WIN_ROWS)
                    table[kind, pair, 0, at_rows, :] = jnp.where(inside & edge, rolled, -jnp.inf)
                    table[kind, pair, 1, at_rows, :] = jnp.where(inside & inner, rolled, -jnp.inf)
        return carry

    last_row = kv.shape[0] - 1
    kv[last_row] = jnp.zeros(kv.shape[1:], jnp.bfloat16)

    @pl.when(z == 0)
    def _():
        kv[0:reach] = jnp.zeros((reach,) + kv.shape[1:], jnp.bfloat16)

    @pl.when(z == n_z - 1)
    def _():
        kv[last_row - reach + 1 : last_row] = jnp.zeros((reach - 1,) + kv.shape[1:], jnp.bfloat16)

    lax.fori_loop(0, pairs // 2, tables, 0)

    value = part[...]
    for k, peer in enumerate(over_sp):
        remote(part, got.at[k], s1.at[k], r1.at[k], (peer, tp)).wait_recv()
        value = value + got[k]
    total[...] = value
    columns = pl.ds(pl.multiple_of(tp * cols, cols), cols)
    full[:, columns] = value
    for k, peer in enumerate(over_tp):
        begin(
            functools.partial(remote, total, full.at[:, columns], s2.at[k], r2.at[k], (sp, peer))
        )
    begin(functools.partial(over_y, g_own, 0, 2))
    last_own = functools.partial(over_y, g_own, 0, 3)
    drain.append((last_own, None))

    @pl.when(same)
    def _():
        last_own().start()

    remote(cs, cx.at[1 - x, ctx_part(c)], s_c.at[0], r_c.at[0], beside).wait_recv()
    ctx_sib = lambda k: remote(
        cx.at[1 - x, ctx_part(k)], cx.at[1 - x, ctx_part(k)], s_c.at[1], r_c.at[1], sib
    )
    begin(lambda: ctx_sib(c))
    lax.fori_loop(pairs // 2, pairs, tables, 0)
    ctx_copy.wait()
    ctx_sib(1 - c).wait_recv()
    for copy in weight_copies:
        copy.wait()
    for k, peer in enumerate(over_tp):
        there = pl.ds(pl.multiple_of(peer * cols, cols), cols)
        remote(total, full.at[:, there], s2.at[k], r2.at[k], (sp, peer)).wait_recv()
    begin(lambda: remote(wo.at[0], wo.at[1], s_w.at[0], r_w.at[0], sib))

    def relay(h):
        from_beside(h).wait_recv()
        over_y(g_x, 1, h).start()
        to_sib(1, g_x, h).start()

    for h in range(chunks):
        drain.append((functools.partial(over_y, g_x, 1, h), None))
        drain.append((functools.partial(to_sib, 1, g_x, h), None))
    relay(0)

    def normed(rows, which):
        rows = rows.astype(jnp.float32)
        inverse = lax.rsqrt(jnp.mean(rows * rows, axis=-1, keepdims=True) + EPSILON)
        lift = gain_ref[...] * (1.0 + full[pl.ds(3 + which, 1), :])
        return (rows * inverse * lift + full[pl.ds(which, 1), :]).astype(jnp.bfloat16)

    hidden = jnp.concatenate([normed(cx[0], 2), normed(cx[1], 2)], axis=0)
    ckv[z] = jnp.dot(hidden, wkv[...], preferred_element_type=jnp.float32).astype(jnp.bfloat16)

    def layer_copy(zb, k, up):
        return remote(ckv.at[zb], ckv.at[zb], s_z.at[k], r_z.at[zb], (sp + 2 * up, tp))

    for k, up in enumerate((2, -2, 1, -1)):
        begin(functools.partial(layer_copy, z, k, up), (z + up >= 0) & (z + up < n_z))
    far_up, far_down = z == n_z - 2, z == 1

    def ctx_relay():
        for cond, zb, k, up in ((far_up, 0, 4, 1), (far_down, n_z - 1, 5, -1)):
            @pl.when(cond)
            def _():
                layer_copy(zb, k, up).wait_recv()
                layer_copy(zb, k, up).start()

    drain.append((functools.partial(layer_copy, 0, 4, 1), far_up))
    drain.append((functools.partial(layer_copy, n_z - 1, 5, -1), far_down))

    g_third = jnp.where(same, g_d, g_y)
    g_fourth = jnp.where(same, g_y, g_d)
    has_up, has_down = z < n_z - 1, z > 0
    halo_up = lambda: remote(
        kv.at[pl.ds(layer_rows, reach)], kv.at[pl.ds(0, reach)], s_h.at[0], r_h.at[0], (sp + 2, tp)
    )
    halo_down = lambda: remote(
        kv.at[pl.ds(reach, reach - 1)], kv.at[pl.ds(reach + layer_rows, reach - 1)],
        s_h.at[1], r_h.at[1], (sp - 2, tp),
    )

    def incoming(k, flow, g, cond):
        @pl.when(cond)
        def _():
            for h in range(chunks):
                over_y(g, flow, h).wait_recv()
                to_sib(k, g, h).start()

    def shared(k, g, cond):
        @pl.when(cond)
        def _():
            for h in range(chunks):
                from_sib(k, g, h).wait_recv()

    for h in range(chunks):
        drain.append((functools.partial(to_sib, 2, g_y, h), None))
        drain.append((functools.partial(to_sib, 3, g_d, h), None))

    def before(k):
        if k == 0:
            for h in range(chunks):
                from_sib(0, g_own, h).wait_recv()
        if k == 1:
            for h in range(1, chunks):
                relay(h)

            @pl.when(differs)
            def _():
                last_own().start()

            for h in range(chunks):
                from_sib(1, g_x, h).wait_recv()
        if k == 2:
            incoming(2, 0, g_y, differs)
            ctx_relay()
            incoming(3, 1, g_d, same)
            shared(2, g_y, differs)
            shared(3, g_d, same)
        if k == 3:
            incoming(2, 0, g_y, same)
            incoming(3, 1, g_d, differs)
            shared(2, g_y, same)
            shared(3, g_d, differs)

    def project(i, carry):
        for k in range(4):
            @pl.when(i == k)
            def _():
                before(k)

        g = jnp.where(i == 0, g_own, jnp.where(i == 1, g_x, jnp.where(i == 2, g_third, g_fourth)))
        hidden = jnp.concatenate([normed(buf[2 * g + e], x) for e in range(2)], axis=0)
        value = jnp.dot(hidden, wkv[...], preferred_element_type=jnp.float32).astype(jnp.bfloat16)
        kv[pl.ds(reach + group_rows * g, group_rows)] = value.reshape(group_rows, GRID_W, 2 * cols)
        query = jnp.dot(hidden, wq[...], preferred_element_type=jnp.float32)
        query = query.reshape(group_rows, GRID_W, cols)
        query = jnp.concatenate([query[:, GRID_W - half :], query[:, : GRID_W - half]], axis=1)
        qs[pl.ds(group_rows * g, group_rows)] = query.astype(jnp.bfloat16)

        @pl.when((g == 0) & has_down)
        def _():
            halo_down().start()

        @pl.when((g == 3) & has_up)
        def _():
            halo_up().start()

        return carry

    lax.fori_loop(0, 4, project, 0)
    drain.append((halo_down, has_down))
    drain.append((halo_up, has_up))

    for k in range(1, n_z):
        zb = lax.rem(z + k, n_z)
        done = (far_up & (zb == 0)) | (far_down & (zb == n_z - 1))

        @pl.when(jnp.logical_not(done))
        def _():
            layer_copy(zb, 0, 1).wait_recv()

    remote(wo.at[0], wo.at[1], s_w.at[0], r_w.at[0], sib).wait_recv()

    factor = HEAD_DIM ** (-0.5) * LOG2E
    contract = (((1,), (1,)), ((), ()))
    low = lax.broadcasted_iota(jnp.int32, (nq, lanes), 1) < HEAD_DIM
    first_head = lax.broadcasted_iota(jnp.int32, (2 * nq, 1), 0) < nq
    key_rows = nk // span
    ctx_count = ckv.shape[0] * ckv.shape[1]

    def attend(i, g, pair):
        own = pl.ds(pl.multiple_of(pair * lanes, lanes), lanes)
        values_at = pl.ds(pl.multiple_of(cols + pair * lanes, lanes), lanes)
        rows = pl.ds(group_rows * g, key_rows)
        kind = jnp.where(g == 0, 1, jnp.where(g == 3, 2, 0))
        ck = ckv[:, :, own].reshape(ctx_count, lanes)
        cv = ckv[:, :, values_at].reshape(ctx_count, lanes)
        cv = jnp.concatenate([cv, jnp.ones((ctx_count, lanes), jnp.bfloat16)], axis=1)
        ones = jnp.ones((nk, lanes), jnp.bfloat16)
        lift = jnp.where(first_head, far_ref[2 * pair], far_ref[2 * pair + 1]) * LOG2E
        outs = []
        for b in range(GRID_W // WIN_COLS):
            q = qs[pl.ds(group_rows * g, group_rows), WIN_COLS * b : WIN_COLS * (b + 1), own]
            q = q.reshape(nq, lanes)
            zero = jnp.zeros_like(q)
            q = jnp.concatenate([jnp.where(low, q, zero), jnp.where(low, zero, q)], axis=0)

            def keys(part_at):
                if b == 0:
                    got = jnp.concatenate(
                        [kv[rows, GRID_W - WIN_COLS :, part_at], kv[rows, :WIN_COLS, part_at]], axis=1
                    )
                else:
                    got = kv[rows, WIN_COLS * (b - 1) : WIN_COLS * (b + 1), part_at]
                return got.reshape(nk, lanes)

            v = jnp.concatenate([keys(values_at), ones], axis=1)
            near = lax.dot_general(q, keys(own), contract, preferred_element_type=jnp.float32)
            near = near * factor + table[kind, pair, min(b, 1)]
            far = lax.dot_general(q, ck, contract, preferred_element_type=jnp.float32)
            top = jnp.maximum(
                jnp.max(near, axis=-1, keepdims=True),
                jnp.max(far, axis=-1, keepdims=True) * factor + lift,
            )
            near = jnp.exp2(near - top).astype(jnp.bfloat16)
            far = jnp.exp2(far * factor + (lift - top)).astype(jnp.bfloat16)
            summed = jnp.dot(near, v, preferred_element_type=jnp.float32) + jnp.dot(
                far, cv, preferred_element_type=jnp.float32
            )
            mean = summed[:, :lanes] / summed[:, lanes:]
            outs.append(jnp.where(low, mean[:nq], mean[nq:]).reshape(group_rows, WIN_COLS, lanes))
        outs = [outs[0][:, half:]] + outs[1:] + [outs[0][:, :half]]
        att[i, :, :, own] = jnp.concatenate(outs, axis=1).astype(jnp.bfloat16)

    def att_half(i, k):
        return att.at[i, pl.ds(own_rows * k, own_rows)]

    def to_across(i, slot, h):
        part_at = pl.ds(h * size, size)
        return remote(
            parts.at[i, part_at], y_in.at[slot, part_at], s_p.at[slot, h], r_p.at[slot, h], across
        )

    def attention_step(i, carry):
        inner_first = jnp.where(y == 0, 1, 2)
        g = jnp.where(
            i == 0, inner_first, jnp.where(i == 1, 3 - inner_first, jnp.where(i == 2, 3 * (1 - y), 3 * y))
        )

        @pl.when((g == 0) & has_down)
        def _():
            remote(kv.at[pl.ds(0, reach)], kv.at[pl.ds(0, reach)], s_h.at[0], r_h.at[0], (sp - 2, tp)).wait_recv()

        @pl.when((g == 3) & has_up)
        def _():
            there = kv.at[pl.ds(reach + layer_rows, reach - 1)]
            remote(there, there, s_h.at[1], r_h.at[1], (sp + 2, tp)).wait_recv()

        def one(pair, inner_carry):
            attend(i, g, pair)
            return inner_carry

        lax.fori_loop(0, pairs, one, 0)
        give = remote(att_half(i, 1 - c), att_in.at[i], s_a.at[i], r_a.at[i], sib)
        give.start()
        update = jnp.dot(
            att[i, pl.ds(own_rows * c, own_rows)].reshape(tokens, cols), wo[0],
            preferred_element_type=jnp.float32,
        )
        give.wait_recv()
        update = update + jnp.dot(
            att_in[i].reshape(tokens, cols), wo[1], preferred_element_type=jnp.float32
        )
        parts[i] = update.astype(jnp.bfloat16)
        for slot in range(2):
            @pl.when(i == 2 * slot)
            def _():
                for h in range(chunks):
                    to_across(2 * slot, slot, h).start()

        return carry

    lax.fori_loop(0, 4, attention_step, 0)
    to_att = lambda i: remote(att_half(i, 1 - c), att_in.at[i], s_a.at[i], r_a.at[i], sib)
    for i in range(4):
        drain.append((functools.partial(to_att, i), None))

    def to_owner(h):
        part_at = pl.ds(h * size, size)
        return remote(fwd.at[part_at], x_in.at[part_at], s_f.at[h], r_f.at[h], beside)

    def finish(which, h, base, update):
        gate = full[pl.ds(6 + which, 1), :]
        out_ref[which, pl.ds(h * size, size)] = (base.astype(jnp.float32) + gate * update).astype(jnp.bfloat16)

    for slot in range(2):
        final, onward = (differs, same) if slot == 0 else (same, differs)
        for h in range(chunks):
            part_at = pl.ds(h * size, size)
            to_across(2 * slot, slot, h).wait_recv()

            @pl.when(onward)
            def _():
                both = parts[2 * slot + 1, part_at].astype(jnp.float32) + y_in[slot, part_at].astype(jnp.float32)
                fwd[part_at] = both.astype(jnp.bfloat16)
                to_owner(h).start()

            @pl.when(final)
            def _():
                both = parts[2 * slot + 1, part_at].astype(jnp.float32) + y_in[slot, part_at].astype(jnp.float32)
                finish(x, h, buf[2 * g_own + c, part_at], both)

            drain.append((functools.partial(to_across, 2 * slot, slot, h), None))
    for h in range(chunks):
        part_at = pl.ds(h * size, size)
        to_owner(h).wait_recv()
        finish(1 - x, h, other[part_at], x_in[part_at].astype(jnp.float32))
        drain.append((functools.partial(to_owner, h), None))

    for make, cond in drain:
        if cond is None:
            make().wait_send()
        else:
            @pl.when(cond)
            def _():
                make().wait_send()


def on_eight(
    latent, context, cond, ctx_cond, w_shift, w_scale, w_gate, norm_gain,
    w_query, w_key, w_value, w_out, rel_bias, ctx_bias,
):
    n_sp, n_tp = lax.axis_size("sp"), lax.axis_size("tp")
    samples, tokens, width = latent.shape
    ctx_tokens = context.shape[1]
    rows_mod, cols = w_shift.shape
    heads = cols // HEAD_DIM
    pairs = heads // 2
    n_z = n_sp // 2
    own_rows = tokens // GRID_W
    group_rows = 2 * own_rows
    layer_rows = 4 * group_rows
    key_rows = group_rows + WIN_ROWS
    nq, nk = group_rows * WIN_COLS, key_rows * 2 * WIN_COLS
    flat = jnp.pad(rel_bias, ((0, 0), (0, 1), (0, 1))).reshape(heads, -1)
    vmem, hbm = pl.BlockSpec(memory_space=pltpu.VMEM), pl.BlockSpec(memory_space=pl.ANY)
    dma = pltpu.SemaphoreType.DMA
    chunks = 4
    bf16, f32 = jnp.bfloat16, jnp.float32
    mods = (8, cols)
    return pl.pallas_call(
        block_kernel,
        out_shape=jax.ShapeDtypeStruct(latent.shape, bf16),
        in_specs=[pl.BlockSpec(memory_space=pltpu.SMEM)] + [vmem] * 4 + [hbm] * 9,
        out_specs=vmem,
        scratch_shapes=[
            pltpu.VMEM((8, rows_mod), f32),
            pltpu.VMEM((3, rows_mod, cols), bf16),
            pltpu.VMEM(mods, f32),
            pltpu.VMEM((n_sp - 1,) + mods, f32),
            pltpu.VMEM(mods, f32),
            pltpu.VMEM((8, width), f32),
            pltpu.VMEM((8, tokens, width), bf16),
            pltpu.VMEM((tokens, width), bf16),
            pltpu.VMEM((2, ctx_tokens, width), bf16),
            pltpu.VMEM((ctx_tokens // 2, width), bf16),
            pltpu.VMEM((width, cols), bf16),
            pltpu.VMEM((width, 2 * cols), bf16),
            pltpu.VMEM((2, cols, width), bf16),
            pltpu.VMEM((layer_rows + WIN_ROWS, GRID_W, 2 * cols), bf16),
            pltpu.VMEM((layer_rows, GRID_W, cols), bf16),
            pltpu.VMEM((n_z, 2 * ctx_tokens, 2 * cols), bf16),
            pltpu.VMEM((3, pairs, 2, 2 * nq, nk), f32),
            pltpu.VMEM((4, group_rows, GRID_W, cols), bf16),
            pltpu.VMEM((4, own_rows, GRID_W, cols), bf16),
            pltpu.VMEM((4, tokens, width), bf16),
            pltpu.VMEM((2, tokens, width), bf16),
            pltpu.VMEM((tokens, width), bf16),
            pltpu.VMEM((tokens, width), bf16),
            dma((11,)),
            dma((n_sp - 1,)), dma((n_sp - 1,)), dma((n_tp - 1,)), dma((n_tp - 1,)),
            dma((2,)), dma((2,)), dma((chunks,)), dma((chunks,)),
            dma((2, chunks)), dma((2, chunks)), dma((4, chunks)), dma((4, chunks)),
            dma((6,)), dma((n_z,)), dma((2,)), dma((2,)),
            dma((1,)), dma((1,)), dma((4,)), dma((4,)),
            dma((2, chunks)), dma((2, chunks)), dma((chunks,)), dma((chunks,)),
        ],
        compiler_params=pltpu.CompilerParams(
            collective_id=1, has_side_effects=True, vmem_limit_bytes=60 * 2**20
        ),
    )(
        ctx_bias, flat, norm_gain[None, :], cond, ctx_cond[None, :],
        w_shift, w_scale, w_gate, latent, context, w_query, w_key, w_value, w_out,
    )


def solution(mesh):
    shape = dict(mesh.shape)
    quick = shape["tp"] == 4 and shape["sp"] == 8
    return jax.shard_map(
        on_eight if quick else on_device,
        mesh=mesh,
        in_specs=(
            P(None, ("sp", "tp"), None),
            P(None, "sp", None),
            P(),
            P(),
            P("sp", "tp"),
            P("sp", "tp"),
            P("sp", "tp"),
            P(),
            P(None, "tp"),
            P(None, "tp"),
            P(None, "tp"),
            P("tp", None),
            P("tp", None, None),
            P("tp"),
        ),
        out_specs=P(None, ("sp", "tp"), None),
        check_vma=False,
    )
```

time: 140 us -> 90.4 us (0.65)
  Pallas kernels: 130 us -> 85 us
  matrix products: 2.34 us -> 0 us
  other arithmetic: 2.01 us -> 0 us
    pallas_call x3 -> x1, Pallas kernels: 130 us -> 85 us  [on_eight(): pl.pallas_call(block_kernel, out_shape=jax.ShapeDtypeStruct(latent.shape,...]
    dot_general x1 -> x0, matrix products: 2.34 us -> none  [on_four(): jnp.dot(attended, w_out, preferred_element_type=jnp.float32)]
    unnamed x5 -> x2, local copies, waits for them, and re-layouts: 0.85 us -> 3.15 us
    convert_element_type x3 -> x0, other arithmetic: 2.01 us -> none  [the longest x1 1.28 us: on_four(): return (latent.astype(jnp.float32) + gate * update).astype(jnp.bfloat16)]
where the time goes in v1:
time: 90.4 us; the launch traced here: 90.1 us
  Pallas kernels  85 us (94%)
  local copies, waits for them, and re-layouts  5.13 us (6%)
    pallas_call x1, Pallas kernels, on_eight(): pl.pallas_call(block_kernel, out_shape=jax.ShapeDtypeStruct(latent.shape,...  85 us
    unnamed x2, local copies, waits for them, and re-layouts  3.15 us

profile of v1, /device:TPU:0, one launch (start us, length us, event | category | flops | bytes accessed | tf_op | source)
XLA Modules:
  0.0 90.1 jit_solution(10659828329672127711)
XLA Ops:
  0.0 1.3 %broadcast_in_dim.7.ctx_cond_ref = bf16[1,2048]{1,0:T(2,128)(2,1)} reshape(bf16[2048]{0:T(1024)(128)(2,1)} %param.17) | data formatting | bytes 8192 | tf_op jit(solution)/shard_map/broadcast_in_dim | solution.py:763
  1.3 0.8 copy.16
  2.1 0.7 reshape.3.flat_ref
  2.8 85.0 %shard_map.136 = bf16[2,128,2048]{2,1,0:T(8,128)(2,1)} custom-call(f32[8]{0:T(128)} %far_ref.1, f32[8,512]{1,0:T(8,128)} %reshape.3.flat_ref, f32[1,2048]{1,0:T(1,128)} %bitcast.1, bf16[2,2048]{1,0:T(2,128)(2,1)} %cond_ref.1, bf16[1,2048]{1,0:T(2,128)(2,1)} %broadcast_in_dim.7.ctx_cond_ref, bf16[256,512]{1,0:T(8,128)(2,1)} %ws_ref.1, ...), custom_call_target="tpu_custom_call" | custom-call | tf_op jit(solution)/shard_map/pallas_call | solution.py:722
  87.8 2.3 %copy.18 = bf16[2,128,2048]{2,1,0:T(8,128)(2,1)} copy(bf16[2,128,2048]{2,1,0:T(8,128)(2,1)} %shard_map.136) | data formatting | bytes 2097152
  (1 shorter events, 0.0 us)

commit v2 on v1

--- a/solution.py
+++ b/solution.py
@@ -234,10 +234,10 @@
 
 
 def block_kernel(
-    far_ref, flat_ref, gain_ref, cond_ref, ctx_cond_ref,
+    far_ref, bias_ref, gain_ref, cond_ref, ctx_cond_ref,
     ws_ref, wc_ref, wg_ref, latent_ref, ctx_ref, wq_ref, wk_ref, wv_ref, wo_ref,
     out_ref,
-    ada, wm, part, got, total, full, buf, other, cx, cs, wq, wkv, wo, kv, qs, ckv, table,
+    flat, ada, wm, part, got, total, full, buf, other, cx, cs, wq, wkv, wo, kv, qs, ckv, table,
     att, att_in, parts, y_in, fwd, x_in,
     own_sem, s1, r1, s2, r2, s_c, r_c, s_x, r_x, s_y, r_y, s_d, r_d, s_z, r_z, s_h, r_h,
     s_w, r_w, s_a, r_a, s_p, r_p, s_f, r_f,
@@ -324,7 +324,13 @@
     mine = pl.ds(pl.multiple_of(sp * rows_mod, rows_mod), rows_mod)
     ada[...] = jnp.zeros_like(ada)
     ada[0:2, :] = cond_ref[:, mine].astype(jnp.float32)
-    ada[2:3, :] = ctx_cond_ref[:, mine].astype(jnp.float32)
+    ctx_cond = ctx_cond_ref[...].astype(jnp.float32)
+    for k in range(n_sp):
+        @pl.when(sp == k)
+        def _():
+            for j in range(rows_mod // 128):
+                line = k * (rows_mod // 128) + j
+                ada[2:3, 128 * j : 128 * (j + 1)] = ctx_cond[line : line + 1, :]
     values = ada[...]
     values = (values / (1.0 + jnp.exp(-values))).astype(jnp.bfloat16)
     at = 0
@@ -357,9 +363,13 @@
     inner = (k_col - p >= 0) & (k_col - p < WIN_COLS)
     edge = (p < half) == (k_col < WIN_COLS)
 
+    flat[...] = jnp.zeros_like(flat)
+    for k in range(bias_ref.shape[0]):
+        flat[:, span * k : span * k + bias_ref.shape[2]] = bias_ref[k]
+
     def tables(pair, carry):
         for h in range(2):
-            line = flat_ref[pl.ds(2 * pair + h, 1), :]
+            line = flat[pl.ds(2 * pair + h, 1), :]
             line = jnp.broadcast_to(line, (WIN_COLS, line.shape[1]))
             for r in range(group_rows):
                 shift = (span * (r + reach - WIN_ROWS + 1) - half + 1) % line.shape[1]
@@ -448,6 +458,7 @@
     for k, up in enumerate((2, -2, 1, -1)):
         begin(functools.partial(layer_copy, z, k, up), (z + up >= 0) & (z + up < n_z))
     far_up, far_down = z == n_z - 2, z == 1
+    relays = far_up | far_down
 
     def ctx_relay():
         for cond, zb, k, up in ((far_up, 0, 4, 1), (far_down, n_z - 1, 5, -1)):
@@ -503,11 +514,20 @@
                 from_sib(1, g_x, h).wait_recv()
         if k == 2:
             incoming(2, 0, g_y, differs)
-            ctx_relay()
             incoming(3, 1, g_d, same)
             shared(2, g_y, differs)
             shared(3, g_d, same)
         if k == 3:
+            ctx_relay()
+
+            @pl.when(relays & has_down)
+            def _():
+                halo_down().start()
+
+            @pl.when(relays & has_up)
+            def _():
+                halo_up().start()
+
             incoming(2, 0, g_y, same)
             incoming(3, 1, g_d, differs)
             shared(2, g_y, same)
@@ -528,11 +548,11 @@
         query = jnp.concatenate([query[:, GRID_W - half :], query[:, : GRID_W - half]], axis=1)
         qs[pl.ds(group_rows * g, group_rows)] = query.astype(jnp.bfloat16)
 
-        @pl.when((g == 0) & has_down)
+        @pl.when((g == 0) & has_down & jnp.logical_not(relays))
         def _():
             halo_down().start()
 
-        @pl.when((g == 3) & has_up)
+        @pl.when((g == 3) & has_up & jnp.logical_not(relays))
         def _():
             halo_up().start()
 
@@ -559,9 +579,9 @@
     key_rows = nk // span
     ctx_count = ckv.shape[0] * ckv.shape[1]
 
-    def attend(i, g, pair):
-        own = pl.ds(pl.multiple_of(pair * lanes, lanes), lanes)
-        values_at = pl.ds(pl.multiple_of(cols + pair * lanes, lanes), lanes)
+    def attend(i, g, pair, blocks):
+        own = pl.ds(pair * lanes, lanes)
+        values_at = pl.ds(cols + pair * lanes, lanes)
         rows = pl.ds(group_rows * g, key_rows)
         kind = jnp.where(g == 0, 1, jnp.where(g == 3, 2, 0))
         ck = ckv[:, :, own].reshape(ctx_count, lanes)
@@ -569,8 +589,7 @@
         cv = jnp.concatenate([cv, jnp.ones((ctx_count, lanes), jnp.bfloat16)], axis=1)
         ones = jnp.ones((nk, lanes), jnp.bfloat16)
         lift = jnp.where(first_head, far_ref[2 * pair], far_ref[2 * pair + 1]) * LOG2E
-        outs = []
-        for b in range(GRID_W // WIN_COLS):
+        for b in blocks:
             q = qs[pl.ds(group_rows * g, group_rows), WIN_COLS * b : WIN_COLS * (b + 1), own]
             q = q.reshape(nq, lanes)
             zero = jnp.zeros_like(q)
@@ -599,12 +618,15 @@
                 far, cv, preferred_element_type=jnp.float32
             )
             mean = summed[:, :lanes] / summed[:, lanes:]
-            outs.append(jnp.where(low, mean[:nq], mean[nq:]).reshape(group_rows, WIN_COLS, lanes))
-        outs = [outs[0][:, half:]] + outs[1:] + [outs[0][:, :half]]
-        att[i, :, :, own] = jnp.concatenate(outs, axis=1).astype(jnp.bfloat16)
-
-    def att_half(i, k):
-        return att.at[i, pl.ds(own_rows * k, own_rows)]
+            mean = jnp.where(low, mean[:nq], mean[nq:]).reshape(group_rows, WIN_COLS, lanes)
+            att[i, :, WIN_COLS * b : WIN_COLS * (b + 1), own] = mean.astype(jnp.bfloat16)
+
+    def give(i, batch, begins, count):
+        at = pl.ds(begins, count)
+        return remote(
+            att.at[i, pl.ds(own_rows * (1 - c), own_rows), at], att_in.at[i, :, at],
+            s_a.at[batch], r_a.at[batch], sib,
+        )
 
     def to_across(i, slot, h):
         part_at = pl.ds(h * size, size)
@@ -612,81 +634,112 @@
             parts.at[i, part_at], y_in.at[slot, part_at], s_p.at[slot, h], r_p.at[slot, h], across
         )
 
-    def attention_step(i, carry):
-        inner_first = jnp.where(y == 0, 1, 2)
-        g = jnp.where(
-            i == 0, inner_first, jnp.where(i == 1, 3 - inner_first, jnp.where(i == 2, 3 * (1 - y), 3 * y))
-        )
-
-        @pl.when((g == 0) & has_down)
-        def _():
-            remote(kv.at[pl.ds(0, reach)], kv.at[pl.ds(0, reach)], s_h.at[0], r_h.at[0], (sp - 2, tp)).wait_recv()
-
-        @pl.when((g == 3) & has_up)
-        def _():
-            there = kv.at[pl.ds(reach + layer_rows, reach - 1)]
-            remote(there, there, s_h.at[1], r_h.at[1], (sp + 2, tp)).wait_recv()
-
-        def one(pair, inner_carry):
-            attend(i, g, pair)
-            return inner_carry
-
-        lax.fori_loop(0, pairs, one, 0)
-        give = remote(att_half(i, 1 - c), att_in.at[i], s_a.at[i], r_a.at[i], sib)
-        give.start()
-        update = jnp.dot(
-            att[i, pl.ds(own_rows * c, own_rows)].reshape(tokens, cols), wo[0],
-            preferred_element_type=jnp.float32,
-        )
-        give.wait_recv()
-        update = update + jnp.dot(
-            att_in[i].reshape(tokens, cols), wo[1], preferred_element_type=jnp.float32
-        )
-        parts[i] = update.astype(jnp.bfloat16)
-        for slot in range(2):
-            @pl.when(i == 2 * slot)
-            def _():
-                for h in range(chunks):
-                    to_across(2 * slot, slot, h).start()
-
-        return carry
-
-    lax.fori_loop(0, 4, attention_step, 0)
-    to_att = lambda i: remote(att_half(i, 1 - c), att_in.at[i], s_a.at[i], r_a.at[i], sib)
-    for i in range(4):
-        drain.append((functools.partial(to_att, i), None))
-
     def to_owner(h):
         part_at = pl.ds(h * size, size)
         return remote(fwd.at[part_at], x_in.at[part_at], s_f.at[h], r_f.at[h], beside)
 
-    def finish(which, h, base, update):
-        gate = full[pl.ds(6 + which, 1), :]
-        out_ref[which, pl.ds(h * size, size)] = (base.astype(jnp.float32) + gate * update).astype(jnp.bfloat16)
-
-    for slot in range(2):
-        final, onward = (differs, same) if slot == 0 else (same, differs)
+    def sum_at(i, slot, h):
+        part_at = pl.ds(h * size, size)
+        return parts[i, part_at].astype(jnp.float32) + y_in[slot, part_at].astype(jnp.float32)
+
+    def forward(slot):
         for h in range(chunks):
-            part_at = pl.ds(h * size, size)
-            to_across(2 * slot, slot, h).wait_recv()
-
-            @pl.when(onward)
-            def _():
-                both = parts[2 * slot + 1, part_at].astype(jnp.float32) + y_in[slot, part_at].astype(jnp.float32)
-                fwd[part_at] = both.astype(jnp.bfloat16)
-                to_owner(h).start()
-
-            @pl.when(final)
-            def _():
-                both = parts[2 * slot + 1, part_at].astype(jnp.float32) + y_in[slot, part_at].astype(jnp.float32)
-                finish(x, h, buf[2 * g_own + c, part_at], both)
-
-            drain.append((functools.partial(to_across, 2 * slot, slot, h), None))
+            to_across(slot, slot, h).wait_recv()
+            fwd[pl.ds(h * size, size)] = sum_at(2, slot, h).astype(jnp.bfloat16)
+            to_owner(h).start()
+
+    def group_of(i):
+        first = jnp.where(y == 0, 1, 2)
+        return jnp.where(i == 0, first, jnp.where(i == 1, 3 * (1 - y), jnp.where(i == 2, g_x, g_own)))
+
+    def attention_block(i, batch, begins, count):
+        g = group_of(i)
+        blocks = range(begins // WIN_COLS, (begins + count) // WIN_COLS)
+
+        for pair in range(pairs):
+            attend(i, g, pair, blocks)
+        give(i, batch, begins, count).start()
+        at = pl.ds(begins, count)
+        update = jnp.dot(
+            att[i, pl.ds(own_rows * c, own_rows), at].reshape(own_rows * count, cols), wo[0],
+            preferred_element_type=jnp.float32,
+        )
+        give(i, batch, begins, count).wait_recv()
+        update = update + jnp.dot(
+            att_in[i, :, at].reshape(own_rows * count, cols), wo[1], preferred_element_type=jnp.float32
+        )
+        for r in range(own_rows):
+            parts[i, GRID_W * r + begins : GRID_W * r + begins + count] = update[
+                count * r : count * (r + 1)
+            ].astype(jnp.bfloat16)
+
+    for part_of in range(2):
+        attention_block(0, part_of, size * part_of, size)
+        for r in range(own_rows):
+            to_across(0, 0, 2 * r + part_of).start()
+
+    def attention_step(i, carry):
+        g = group_of(i)
+
+        @pl.when((g == 0) & has_down)
+        def _():
+            there = kv.at[pl.ds(0, reach)]
+            remote(there, there, s_h.at[0], r_h.at[0], (sp - 2, tp)).wait_recv()
+
+        @pl.when((g == 3) & has_up)
+        def _():
+            there = kv.at[pl.ds(reach + layer_rows, reach - 1)]
+            remote(there, there, s_h.at[1], r_h.at[1], (sp + 2, tp)).wait_recv()
+
+        attention_block(i, i + 1, 0, GRID_W)
+
+        @pl.when(i == 1)
+        def _():
+            for h in range(chunks):
+                to_across(1, 1, h).start()
+
+        @pl.when((i == 2) & same)
+        def _():
+            forward(0)
+
+        return carry
+
+    lax.fori_loop(1, 4, attention_step, 0)
+    for part_of in range(2):
+        drain.append((functools.partial(give, 0, part_of, size * part_of, size), None))
+    for i in range(1, 4):
+        drain.append((functools.partial(give, i, i + 1, 0, GRID_W), None))
+
+    def finish(which, h, update):
+        value = full[pl.ds(6 + which, 1), :] * update
+        if h % 2 == 0:
+            row = GRID_W * (h // 2)
+            out_ref[which, row + GRID_W - half : row + GRID_W] = value[:half]
+            out_ref[which, row : row + size - half] = value[half:]
+        else:
+            row = GRID_W * (h // 2) + size - half
+            out_ref[which, row : row + size] = value
+
+    def own(slot):
+        for h in range(chunks):
+            to_across(slot, slot, h).wait_recv()
+            finish(x, h, sum_at(3, slot, h))
+
+    @pl.when(differs)
+    def _():
+        forward(1)
+        own(0)
+
+    @pl.when(same)
+    def _():
+        own(1)
+
     for h in range(chunks):
-        part_at = pl.ds(h * size, size)
         to_owner(h).wait_recv()
-        finish(1 - x, h, other[part_at], x_in[part_at].astype(jnp.float32))
+        finish(1 - x, h, x_in[h * size : (h + 1) * size].astype(jnp.float32))
         drain.append((functools.partial(to_owner, h), None))
+        for slot in range(2):
+            drain.append((functools.partial(to_across, slot, slot, h), None))
 
     for make, cond in drain:
         if cond is None:
@@ -713,18 +766,18 @@
     layer_rows = 4 * group_rows
     key_rows = group_rows + WIN_ROWS
     nq, nk = group_rows * WIN_COLS, key_rows * 2 * WIN_COLS
-    flat = jnp.pad(rel_bias, ((0, 0), (0, 1), (0, 1))).reshape(heads, -1)
-    vmem, hbm = pl.BlockSpec(memory_space=pltpu.VMEM), pl.BlockSpec(memory_space=pl.ANY)
+    vmem, hbm = pl.BlockSpec(memory_space=pltpu.VMEM), pl.BlockSpec(memory_space=pltpu.HBM)
     dma = pltpu.SemaphoreType.DMA
     chunks = 4
     bf16, f32 = jnp.bfloat16, jnp.float32
     mods = (8, cols)
-    return pl.pallas_call(
+    delta = pl.pallas_call(
         block_kernel,
-        out_shape=jax.ShapeDtypeStruct(latent.shape, bf16),
+        out_shape=jax.ShapeDtypeStruct(latent.shape, f32),
         in_specs=[pl.BlockSpec(memory_space=pltpu.SMEM)] + [vmem] * 4 + [hbm] * 9,
         out_specs=vmem,
         scratch_shapes=[
+            pltpu.VMEM((heads, 2 * WIN_ROWS * 2 * WIN_COLS), f32),
             pltpu.VMEM((8, rows_mod), f32),
             pltpu.VMEM((3, rows_mod, cols), bf16),
             pltpu.VMEM(mods, f32),
@@ -753,16 +806,22 @@
             dma((2,)), dma((2,)), dma((chunks,)), dma((chunks,)),
             dma((2, chunks)), dma((2, chunks)), dma((4, chunks)), dma((4, chunks)),
             dma((6,)), dma((n_z,)), dma((2,)), dma((2,)),
-            dma((1,)), dma((1,)), dma((4,)), dma((4,)),
+            dma((1,)), dma((1,)), dma((5,)), dma((5,)),
             dma((2, chunks)), dma((2, chunks)), dma((chunks,)), dma((chunks,)),
         ],
         compiler_params=pltpu.CompilerParams(
-            collective_id=1, has_side_effects=True, vmem_limit_bytes=60 * 2**20
+            collective_id=1, has_side_effects=True, vmem_limit_bytes=48 * 2**20
         ),
     )(
-        ctx_bias, flat, norm_gain[None, :], cond, ctx_cond[None, :],
-        w_shift, w_scale, w_gate, latent, context, w_query, w_key, w_value, w_out,
+        *[
+            pltpu.with_memory_space_constraint(v, pltpu.HBM)
+            for v in (
+                ctx_bias, rel_bias.transpose(1, 0, 2), norm_gain[None, :], cond, ctx_cond.reshape(-1, 128),
+                w_shift, w_scale, w_gate, latent, context, w_query, w_key, w_value, w_out,
+            )
+        ]
     )
+    return (latent.astype(f32) + delta).astype(bf16)
 
 
 def solution(mesh):

time: 90.4 us -> 78.6 us (0.87)
  Pallas kernels: 85 us -> 77.2 us
  local copies, waits for them, and re-layouts: 5.13 us -> 0.01 us
  other arithmetic: 0 us -> 1.26 us
    pallas_call x1, Pallas kernels: 85 us -> 77.2 us  [on_eight(): pl.pallas_call(block_kernel, out_shape=jax.ShapeDtypeStruct(latent.shape,...]
    unnamed x2, local copies, waits for them, and re-layouts: 3.15 us -> 0.01 us
    broadcast_in_dim x1 -> x0, local copies, waits for them, and re-layouts: 1.28 us -> none  [on_eight(): ctx_cond[None, :]]
    convert_element_type x0 -> x1, other arithmetic: none -> 1.26 us  [on_eight(): return (latent.astype(f32) + delta).astype(bf16)]
where the time goes in v2:
time: 78.6 us; the launch traced here: 78.5 us
  Pallas kernels  77.2 us (98%)
  other arithmetic  1.26 us (2%)
    pallas_call x1, Pallas kernels, on_eight(): pl.pallas_call(block_kernel, out_shape=jax.ShapeDtypeStruct(latent.shape,...  77.2 us

profile of v2, /device:TPU:0, one launch (start us, length us, event | category | flops | bytes accessed | tf_op | source)
XLA Modules:
  0.0 78.5 jit_solution(7526482671005543306)
XLA Ops:
  0.0 0.0 copy-start
  0.0 77.2 %shard_map.136 = f32[2,128,2048]{2,1,0:T(8,128)S(1)} custom-call(f32[8]{0:T(128)} %far_ref.1, f32[15,8,31]{2,1,0:T(8,128)} %bitcast.3, f32[1,2048]{1,0:T(1,128)} %bitcast.4, bf16[2,2048]{1,0:T(2,128)(2,1)} %cond_ref.1, bf16[16,128]{1,0:T(8,128)(2,1)} %bitcast.5, bf16[256,512]{1,0:T(8,128)(2,1)} %ws_ref.1, bf16[256,512]{1,0:T(8,128)(2,1)} %wc_ref.1, ...), custom_call_target="tpu_custom_call" | custom-call | tf_op jit(solution)/shard_map/pallas_call | solution.py:774
  77.2 0.0 copy-done
  77.2 1.3 %add_convert_fusion = bf16[2,128,2048]{2,1,0:T(8,128)(2,1)} fusion(f32[2,128,2048]{2,1,0:T(8,128)S(1)} %shard_map.136, bf16[2,128,2048]{2,1,0:T(8,128)(2,1)S(1)} %copy-done), kind=kLoop, calls=%fused_computation | loop fusion | flops 1572864 | bytes 4194304 | tf_op jit(solution)/shard_map/convert_element_type | solution.py:824
Async XLA Ops:
  0.0 77.2 %copy-start = (bf16[2,128,2048]{2,1,0:T(8,128)(2,1)S(1)}, bf16[2,128,2048]{2,1,0:T(8,128)(2,1)}, u32[]{:S(2)}) copy-start(bf16[2,128,2048]{2,1,0:T(8,128)(2,1)} %latent_ref.1) | copy-start | bytes 3145732

commit v3 on v2

--- a/solution.py
+++ b/solution.py
@@ -226,17 +226,11 @@
 MESH = pl.DeviceIdType.MESH
 
 
-def entry_barrier(peers):
-    barrier = pltpu.get_barrier_semaphore()
-    for device in peers:
-        pl.semaphore_signal(barrier, inc=1, device_id=device, device_id_type=MESH)
-    pl.semaphore_wait(barrier, len(peers))
-
-
 def block_kernel(
-    far_ref, bias_ref, gain_ref, cond_ref, ctx_cond_ref,
+    far_hbm, bias_hbm, gain_hbm, cond_hbm, ctx_cond_hbm,
     ws_ref, wc_ref, wg_ref, latent_ref, ctx_ref, wq_ref, wk_ref, wv_ref, wo_ref,
     out_ref,
+    far_ref, bias_ref, gain_ref, cond_ref, ctx_cond_ref, acc,
     flat, ada, wm, part, got, total, full, buf, other, cx, cs, wq, wkv, wo, kv, qs, ckv, table,
     att, att_in, parts, y_in, fwd, x_in,
     own_sem, s1, r1, s2, r2, s_c, r_c, s_x, r_x, s_y, r_y, s_d, r_d, s_z, r_z, s_h, r_h,
@@ -287,6 +281,13 @@
         copy.start()
         return copy
 
+    small_copies = [
+        local(11 + k, src, dst)
+        for k, (src, dst) in enumerate((
+            (cond_hbm, cond_ref), (ctx_cond_hbm, ctx_cond_ref), (bias_hbm, bias_ref),
+            (gain_hbm, gain_ref), (far_hbm, far_ref),
+        ))
+    ]
     mod_copies = [local(k, w, wm.at[k]) for k, w in enumerate((ws_ref, wc_ref, wg_ref))]
     other_copy = local(3, latent_ref.at[1 - x], other)
     own_copy = local(4, latent_ref.at[x], buf.at[2 * g_own + c])
@@ -300,7 +301,10 @@
         local(9, wq_ref, wq),
         local(10, wo_ref, wo.at[0]),
     ]
-    entry_barrier([(p, tp) for p in over_sp] + [(sp, p) for p in over_tp])
+    barrier = pltpu.get_barrier_semaphore()
+    peers = [(p, tp) for p in over_sp] + [(sp, p) for p in over_tp]
+    for device in peers:
+        pl.semaphore_signal(barrier, inc=1, device_id=device, device_id_type=MESH)
 
     def piece(g, h):
         return buf.at[2 * g + c, pl.ds(h * size, size)]
@@ -322,6 +326,8 @@
         return remote(there, there, s_d.at[k, h], r_d.at[k, h], sib)
 
     mine = pl.ds(pl.multiple_of(sp * rows_mod, rows_mod), rows_mod)
+    small_copies[0].wait()
+    small_copies[1].wait()
     ada[...] = jnp.zeros_like(ada)
     ada[0:2, :] = cond_ref[:, mine].astype(jnp.float32)
     ctx_cond = ctx_cond_ref[...].astype(jnp.float32)
@@ -339,15 +345,17 @@
         value = jnp.dot(values, wm[k], preferred_element_type=jnp.float32)
         part[at : at + count, :] = value[:count]
         at += count
+    stage_copy.wait()
+    other_copy.wait()
+    own_copy.wait()
+    pl.semaphore_wait(barrier, len(peers))
     for k, peer in enumerate(over_sp):
         begin(functools.partial(remote, part, got.at[k], s1.at[k], r1.at[k], (peer, tp)))
 
-    stage_copy.wait()
     begin(lambda: remote(cs, cx.at[x, ctx_part(c)], s_c.at[0], r_c.at[0], beside))
-    other_copy.wait()
-    own_copy.wait()
+    upfront, between = 3 * chunks // 8, 5 * chunks // 8
     for h in range(chunks):
-        if h < 2:
+        if h < upfront:
             begin(functools.partial(over_y, g_own, 0, h))
         begin(functools.partial(to_beside, h))
     for h in range(chunks):
@@ -363,6 +371,7 @@
     inner = (k_col - p >= 0) & (k_col - p < WIN_COLS)
     edge = (p < half) == (k_col < WIN_COLS)
 
+    small_copies[2].wait()
     flat[...] = jnp.zeros_like(flat)
     for k in range(bias_ref.shape[0]):
         flat[:, span * k : span * k + bias_ref.shape[2]] = bias_ref[k]
@@ -410,13 +419,19 @@
         begin(
             functools.partial(remote, total, full.at[:, columns], s2.at[k], r2.at[k], (sp, peer))
         )
-    begin(functools.partial(over_y, g_own, 0, 2))
-    last_own = functools.partial(over_y, g_own, 0, 3)
-    drain.append((last_own, None))
+    for h in range(upfront, between):
+        begin(functools.partial(over_y, g_own, 0, h))
+
+    def rest_own():
+        for h in range(between, chunks):
+            over_y(g_own, 0, h).start()
+
+    for h in range(between, chunks):
+        drain.append((functools.partial(over_y, g_own, 0, h), None))
 
     @pl.when(same)
     def _():
-        last_own().start()
+        rest_own()
 
     remote(cs, cx.at[1 - x, ctx_part(c)], s_c.at[0], r_c.at[0], beside).wait_recv()
     ctx_sib = lambda k: remote(
@@ -424,25 +439,24 @@
     )
     begin(lambda: ctx_sib(c))
     lax.fori_loop(pairs // 2, pairs, tables, 0)
+    def relay(h):
+        from_beside(h).wait_recv()
+        over_y(g_x, 1, h).start()
+        to_sib(1, g_x, h).start()
+
+    for h in range(chunks):
+        drain.append((functools.partial(over_y, g_x, 1, h), None))
+        drain.append((functools.partial(to_sib, 1, g_x, h), None))
+    relay(0)
     ctx_copy.wait()
     ctx_sib(1 - c).wait_recv()
-    for copy in weight_copies:
+    for copy in weight_copies + small_copies[3:]:
         copy.wait()
     for k, peer in enumerate(over_tp):
         there = pl.ds(pl.multiple_of(peer * cols, cols), cols)
         remote(total, full.at[:, there], s2.at[k], r2.at[k], (sp, peer)).wait_recv()
     begin(lambda: remote(wo.at[0], wo.at[1], s_w.at[0], r_w.at[0], sib))
 
-    def relay(h):
-        from_beside(h).wait_recv()
-        over_y(g_x, 1, h).start()
-        to_sib(1, g_x, h).start()
-
-    for h in range(chunks):
-        drain.append((functools.partial(over_y, g_x, 1, h), None))
-        drain.append((functools.partial(to_sib, 1, g_x, h), None))
-    relay(0)
-
     def normed(rows, which):
         rows = rows.astype(jnp.float32)
         inverse = lax.rsqrt(jnp.mean(rows * rows, axis=-1, keepdims=True) + EPSILON)
@@ -455,8 +469,21 @@
     def layer_copy(zb, k, up):
         return remote(ckv.at[zb], ckv.at[zb], s_z.at[k], r_z.at[zb], (sp + 2 * up, tp))
 
+    layer_sends = []
     for k, up in enumerate((2, -2, 1, -1)):
-        begin(functools.partial(layer_copy, z, k, up), (z + up >= 0) & (z + up < n_z))
+        ahead = (z + up >= 0) & (z + up < n_z)
+        middle = (z > 0) & (z + 1 < n_z - 1) if up > 0 else (z < n_z - 1) & (z - 1 > 0)
+        layer_sends.append((functools.partial(layer_copy, z, k, up), ahead, middle))
+        drain.append((functools.partial(layer_copy, z, k, up), ahead))
+
+    def send_layer(late):
+        for make, ahead, middle in layer_sends:
+            @pl.when(ahead & (middle if late else jnp.logical_not(middle)))
+            def _():
+                make().start()
+
+    send_layer(False)
+    relay(1)
     far_up, far_down = z == n_z - 2, z == 1
     relays = far_up | far_down
 
@@ -503,31 +530,40 @@
             for h in range(chunks):
                 from_sib(0, g_own, h).wait_recv()
         if k == 1:
-            for h in range(1, chunks):
+            for h in range(2, chunks):
                 relay(h)
 
             @pl.when(differs)
             def _():
-                last_own().start()
-
+                rest_own()
+
+            send_layer(True)
+            incoming(2, 0, g_y, differs)
             for h in range(chunks):
                 from_sib(1, g_x, h).wait_recv()
         if k == 2:
-            incoming(2, 0, g_y, differs)
+            ctx_relay()
+
+            @pl.when(relays & has_down & differs & (g_x == 0))
+            def _():
+                halo_down().start()
+
+            @pl.when(relays & has_up & differs & (g_x == 3))
+            def _():
+                halo_up().start()
+
+            @pl.when(relays & has_down & same & (g_own == 0))
+            def _():
+                halo_down().start()
+
+            @pl.when(relays & has_up & same & (g_own == 3))
+            def _():
+                halo_up().start()
+
             incoming(3, 1, g_d, same)
             shared(2, g_y, differs)
             shared(3, g_d, same)
         if k == 3:
-            ctx_relay()
-
-            @pl.when(relays & has_down)
-            def _():
-                halo_down().start()
-
-            @pl.when(relays & has_up)
-            def _():
-                halo_up().start()
-
             incoming(2, 0, g_y, same)
             incoming(3, 1, g_d, differs)
             shared(2, g_y, same)
@@ -548,11 +584,13 @@
         query = jnp.concatenate([query[:, GRID_W - half :], query[:, : GRID_W - half]], axis=1)
         qs[pl.ds(group_rows * g, group_rows)] = query.astype(jnp.bfloat16)
 
-        @pl.when((g == 0) & has_down & jnp.logical_not(relays))
+        open_now = jnp.logical_not(relays) | (i >= 2)
+
+        @pl.when((g == 0) & has_down & open_now)
         def _():
             halo_down().start()
 
-        @pl.when((g == 3) & has_up & jnp.logical_not(relays))
+        @pl.when((g == 3) & has_up & open_now)
         def _():
             halo_up().start()
 
@@ -580,8 +618,8 @@
     ctx_count = ckv.shape[0] * ckv.shape[1]
 
     def attend(i, g, pair, blocks):
-        own = pl.ds(pair * lanes, lanes)
-        values_at = pl.ds(cols + pair * lanes, lanes)
+        own = pl.ds(pl.multiple_of(pair * lanes, lanes), lanes)
+        values_at = pl.ds(pl.multiple_of(cols + pair * lanes, lanes), lanes)
         rows = pl.ds(group_rows * g, key_rows)
         kind = jnp.where(g == 0, 1, jnp.where(g == 3, 2, 0))
         ck = ckv[:, :, own].reshape(ctx_count, lanes)
@@ -629,43 +667,51 @@
         )
 
     def to_across(i, slot, h):
-        part_at = pl.ds(h * size, size)
+        part_at = pl.ds(pl.multiple_of(h * size, size), size)
         return remote(
             parts.at[i, part_at], y_in.at[slot, part_at], s_p.at[slot, h], r_p.at[slot, h], across
         )
 
+    def chunk(h):
+        return pl.ds(pl.multiple_of(h * size, size), size)
+
     def to_owner(h):
-        part_at = pl.ds(h * size, size)
-        return remote(fwd.at[part_at], x_in.at[part_at], s_f.at[h], r_f.at[h], beside)
+        return remote(fwd.at[chunk(h)], x_in.at[chunk(h)], s_f.at[h], r_f.at[h], beside)
 
     def sum_at(i, slot, h):
-        part_at = pl.ds(h * size, size)
-        return parts[i, part_at].astype(jnp.float32) + y_in[slot, part_at].astype(jnp.float32)
-
-    def forward(slot):
-        for h in range(chunks):
-            to_across(slot, slot, h).wait_recv()
-            fwd[pl.ds(h * size, size)] = sum_at(2, slot, h).astype(jnp.bfloat16)
-            to_owner(h).start()
+        return parts[i, chunk(h)].astype(jnp.float32) + y_in[slot, chunk(h)].astype(jnp.float32)
+
+    def forward(slot, h):
+        to_across(slot, slot, h).wait_recv()
+        fwd[chunk(h)] = sum_at(2, slot, h).astype(jnp.bfloat16)
+        to_owner(h).start()
 
     def group_of(i):
         first = jnp.where(y == 0, 1, 2)
         return jnp.where(i == 0, first, jnp.where(i == 1, 3 * (1 - y), jnp.where(i == 2, g_x, g_own)))
 
-    def attention_block(i, batch, begins, count):
+    def attention_block(i, batch, begins, count, between_pairs=None):
         g = group_of(i)
         blocks = range(begins // WIN_COLS, (begins + count) // WIN_COLS)
 
-        for pair in range(pairs):
-            attend(i, g, pair, blocks)
+        if between_pairs is None:
+            for pair in range(pairs):
+                attend(i, g, pair, blocks)
+        else:
+            def one(pair, carry):
+                attend(i, g, pair, blocks)
+                between_pairs(pair)
+                return carry
+
+            lax.fori_loop(0, pairs, one, 0)
         give(i, batch, begins, count).start()
         at = pl.ds(begins, count)
-        update = jnp.dot(
+        acc[: own_rows * count] = jnp.dot(
             att[i, pl.ds(own_rows * c, own_rows), at].reshape(own_rows * count, cols), wo[0],
             preferred_element_type=jnp.float32,
         )
         give(i, batch, begins, count).wait_recv()
-        update = update + jnp.dot(
+        update = acc[: own_rows * count] + jnp.dot(
             att_in[i, :, at].reshape(own_rows * count, cols), wo[1], preferred_element_type=jnp.float32
         )
         for r in range(own_rows):
@@ -673,14 +719,14 @@
                 count * r : count * (r + 1)
             ].astype(jnp.bfloat16)
 
+    per_row = chunks // own_rows
     for part_of in range(2):
-        attention_block(0, part_of, size * part_of, size)
+        attention_block(0, part_of, GRID_W // 2 * part_of, GRID_W // 2)
         for r in range(own_rows):
-            to_across(0, 0, 2 * r + part_of).start()
-
-    def attention_step(i, carry):
-        g = group_of(i)
-
+            for k in range(per_row // 2):
+                to_across(0, 0, per_row * r + per_row // 2 * part_of + k).start()
+
+    def wait_halo(g):
         @pl.when((g == 0) & has_down)
         def _():
             there = kv.at[pl.ds(0, reach)]
@@ -691,6 +737,10 @@
             there = kv.at[pl.ds(reach + layer_rows, reach - 1)]
             remote(there, there, s_h.at[1], r_h.at[1], (sp + 2, tp)).wait_recv()
 
+    def attention_step(i, carry):
+        g = group_of(i)
+
+        wait_halo(g)
         attention_block(i, i + 1, 0, GRID_W)
 
         @pl.when(i == 1)
@@ -698,27 +748,41 @@
             for h in range(chunks):
                 to_across(1, 1, h).start()
 
-        @pl.when((i == 2) & same)
+        return carry
+
+    lax.fori_loop(1, 3, attention_step, 0)
+    early = chunks - 2 - pairs
+
+    @pl.when(same)
+    def _():
+        for h in range(chunks):
+            forward(0, h)
+
+    @pl.when(differs)
+    def _():
+        for h in range(early):
+            forward(1, h)
+
+    def between_pairs(pair):
+        @pl.when(differs)
         def _():
-            forward(0)
-
-        return carry
-
-    lax.fori_loop(1, 4, attention_step, 0)
+            forward(1, early + pair)
+
+    wait_halo(g_own)
+    attention_block(3, 4, 0, GRID_W, between_pairs)
     for part_of in range(2):
-        drain.append((functools.partial(give, 0, part_of, size * part_of, size), None))
+        drain.append((functools.partial(give, 0, part_of, GRID_W // 2 * part_of, GRID_W // 2), None))
     for i in range(1, 4):
         drain.append((functools.partial(give, i, i + 1, 0, GRID_W), None))
 
     def finish(which, h, update):
         value = full[pl.ds(6 + which, 1), :] * update
-        if h % 2 == 0:
-            row = GRID_W * (h // 2)
+        row, place = GRID_W * (h // per_row), size * (h % per_row)
+        if place == 0:
             out_ref[which, row + GRID_W - half : row + GRID_W] = value[:half]
             out_ref[which, row : row + size - half] = value[half:]
         else:
-            row = GRID_W * (h // 2) + size - half
-            out_ref[which, row : row + size] = value
+            out_ref[which, row + place - half : row + place - half + size] = value
 
     def own(slot):
         for h in range(chunks):
@@ -727,7 +791,8 @@
 
     @pl.when(differs)
     def _():
-        forward(1)
+        for h in range(early + pairs, chunks):
+            forward(1, h)
         own(0)
 
     @pl.when(same)
@@ -768,15 +833,21 @@
     nq, nk = group_rows * WIN_COLS, key_rows * 2 * WIN_COLS
     vmem, hbm = pl.BlockSpec(memory_space=pltpu.VMEM), pl.BlockSpec(memory_space=pltpu.HBM)
     dma = pltpu.SemaphoreType.DMA
-    chunks = 4
+    chunks = 8
     bf16, f32 = jnp.bfloat16, jnp.float32
     mods = (8, cols)
     delta = pl.pallas_call(
         block_kernel,
         out_shape=jax.ShapeDtypeStruct(latent.shape, f32),
-        in_specs=[pl.BlockSpec(memory_space=pltpu.SMEM)] + [vmem] * 4 + [hbm] * 9,
+        in_specs=[hbm] * 14,
         out_specs=vmem,
         scratch_shapes=[
+            pltpu.SMEM(ctx_bias.shape, f32),
+            pltpu.VMEM((rel_bias.shape[1], heads, rel_bias.shape[2]), f32),
+            pltpu.VMEM((1, width), f32),
+            pltpu.VMEM(cond.shape, bf16),
+            pltpu.VMEM((width // 128, 128), bf16),
+            pltpu.VMEM((tokens, width), f32),
             pltpu.VMEM((heads, 2 * WIN_ROWS * 2 * WIN_COLS), f32),
             pltpu.VMEM((8, rows_mod), f32),
             pltpu.VMEM((3, rows_mod, cols), bf16),
@@ -801,7 +872,7 @@
             pltpu.VMEM((2, tokens, width), bf16),
             pltpu.VMEM((tokens, width), bf16),
             pltpu.VMEM((tokens, width), bf16),
-            dma((11,)),
+            dma((16,)),
             dma((n_sp - 1,)), dma((n_sp - 1,)), dma((n_tp - 1,)), dma((n_tp - 1,)),
             dma((2,)), dma((2,)), dma((chunks,)), dma((chunks,)),
             dma((2, chunks)), dma((2, chunks)), dma((4, chunks)), dma((4, chunks)),

time: 78.6 us -> 70.8 us (0.901)
  Pallas kernels: 77.2 us -> 69.4 us
    pallas_call x1, Pallas kernels: 77.2 us -> 69.4 us  [on_eight(): pl.pallas_call(block_kernel, out_shape=jax.ShapeDtypeStruct(latent.shape,...]
where the time goes in v3:
time: 70.8 us; the launch traced here: 70.7 us
  Pallas kernels  69.4 us (98%)
  other arithmetic  1.26 us (2%)
    pallas_call x1, Pallas kernels, on_eight(): pl.pallas_call(block_kernel, out_shape=jax.ShapeDtypeStruct(latent.shape,...  69.4 us

profile of v3, /device:TPU:0, one launch (start us, length us, event | category | flops | bytes accessed | tf_op | source)
XLA Modules:
  0.0 70.7 jit_solution(7428907992864676344)
XLA Ops:
  0.0 0.0 copy-start
  0.0 69.4 %shard_map.136 = f32[2,128,2048]{2,1,0:T(8,128)S(1)} custom-call(f32[8]{0:T(128)} %far_hbm.1, f32[15,8,31]{2,1,0:T(8,128)} %bitcast.3, f32[1,2048]{1,0:T(1,128)} %bitcast.4, bf16[2,2048]{1,0:T(2,128)(2,1)} %cond_hbm.1, bf16[16,128]{1,0:T(8,128)(2,1)} %bitcast.5, bf16[256,512]{1,0:T(8,128)(2,1)} %ws_ref.1, bf16[256,512]{1,0:T(8,128)(2,1)} %wc_ref.1, ...), custom_call_target="tpu_custom_call" | custom-call | tf_op jit(solution)/shard_map/pallas_call | solution.py:839
  69.4 0.0 copy-done
  69.4 1.3 %add_convert_fusion = bf16[2,128,2048]{2,1,0:T(8,128)(2,1)} fusion(f32[2,128,2048]{2,1,0:T(8,128)S(1)} %shard_map.136, bf16[2,128,2048]{2,1,0:T(8,128)(2,1)S(1)} %copy-done), kind=kLoop, calls=%fused_computation | loop fusion | flops 1572864 | bytes 4194304 | tf_op jit(solution)/shard_map/convert_element_type | solution.py:895
Async XLA Ops:
  0.0 69.4 %copy-start = (bf16[2,128,2048]{2,1,0:T(8,128)(2,1)S(1)}, bf16[2,128,2048]{2,1,0:T(8,128)(2,1)}, u32[]{:S(2)}) copy-start(bf16[2,128,2048]{2,1,0:T(8,128)(2,1)} %latent_ref.1) | copy-start | bytes 3145732

commit v4 on v3

--- a/solution.py
+++ b/solution.py
@@ -243,6 +243,7 @@
     n_z = n_sp // 2
     same = x == y
     differs = x != y
+    always = sp >= 0
     tokens, width = other.shape
     cols = wq.shape[1]
     rows_mod = wm.shape[1]
@@ -253,7 +254,8 @@
     own_rows = tokens // GRID_W
     group_rows = 2 * own_rows
     layer_rows = 4 * group_rows
-    chunks = s_x.shape[0]
+    chunks = r_x.shape[0]
+    per_row = chunks // own_rows
     size = tokens // chunks
     over_sp = [lax.rem(sp + k, n_sp) for k in range(1, n_sp)]
     over_tp = [lax.rem(tp + k, n_tp) for k in range(1, n_tp)]
@@ -307,23 +309,26 @@
         pl.semaphore_signal(barrier, inc=1, device_id=device, device_id_type=MESH)
 
     def piece(g, h):
-        return buf.at[2 * g + c, pl.ds(h * size, size)]
+        return buf.at[2 * g + c, pl.ds(pl.multiple_of(h * size, size), size)]
 
     def to_beside(h):
-        return remote(other.at[pl.ds(h * size, size)], piece(g_own, h), s_x.at[h], r_x.at[h], beside)
+        return remote(other.at[pl.ds(h * size, size)], piece(g_own, h), s_x.at[0], r_x.at[h], beside)
 
     def from_beside(h):
-        return remote(other.at[pl.ds(h * size, size)], piece(g_x, h), s_x.at[h], r_x.at[h], beside)
+        return remote(other.at[pl.ds(h * size, size)], piece(g_x, h), s_x.at[0], r_x.at[h], beside)
 
     def over_y(g, flow, h):
-        return remote(piece(g, h), piece(g, h), s_y.at[flow, h], r_y.at[flow, h], across)
+        return remote(piece(g, h), piece(g, h), s_y.at[flow], r_y.at[flow, h], across)
 
     def to_sib(k, g, h):
-        return remote(piece(g, h), piece(g, h), s_d.at[k, h], r_d.at[k, h], sib)
-
-    def from_sib(k, g, h):
-        there = buf.at[2 * g + 1 - c, pl.ds(h * size, size)]
-        return remote(there, there, s_d.at[k, h], r_d.at[k, h], sib)
+        return remote(piece(g, h), piece(g, h), s_d.at[k], r_d.at[k, h // per_row], sib)
+
+    def from_sib(k, g, r):
+        there = buf.at[2 * g + 1 - c, pl.ds(pl.multiple_of(GRID_W * r, GRID_W), GRID_W)]
+        return remote(there, there, s_d.at[k], r_d.at[k, r], sib)
+
+    def sent(ref, sem):
+        drain.append((lambda: remote(ref, ref, sem, sem, sib), None))
 
     mine = pl.ds(pl.multiple_of(sp * rows_mod, rows_mod), rows_mod)
     small_copies[0].wait()
@@ -350,16 +355,24 @@
     own_copy.wait()
     pl.semaphore_wait(barrier, len(peers))
     for k, peer in enumerate(over_sp):
-        begin(functools.partial(remote, part, got.at[k], s1.at[k], r1.at[k], (peer, tp)))
+        remote(part, got.at[k], s1.at[0], r1.at[0], (peer, tp)).start()
+    sent(got, s1.at[0])
 
     begin(lambda: remote(cs, cx.at[x, ctx_part(c)], s_c.at[0], r_c.at[0], beside))
     upfront, between = 3 * chunks // 8, 5 * chunks // 8
     for h in range(chunks):
         if h < upfront:
-            begin(functools.partial(over_y, g_own, 0, h))
-        begin(functools.partial(to_beside, h))
+            over_y(g_own, 0, h).start()
+        to_beside(h).start()
     for h in range(chunks):
-        begin(functools.partial(to_sib, 0, g_own, h))
+        to_sib(0, g_own, h).start()
+    sent(other, s_x.at[0])
+    for k in range(2):
+        sent(other, s_y.at[k])
+        sent(other, s_p.at[k])
+    for k in range(4):
+        sent(other, s_d.at[k])
+    sent(fwd, s_f.at[0])
 
     span = 2 * WIN_COLS
     nk = table.shape[-1]
@@ -409,25 +422,21 @@
     lax.fori_loop(0, pairs // 2, tables, 0)
 
     value = part[...]
-    for k, peer in enumerate(over_sp):
-        remote(part, got.at[k], s1.at[k], r1.at[k], (peer, tp)).wait_recv()
+    remote(got, got, s1.at[0], r1.at[0], sib).wait_recv()
+    for k in range(len(over_sp)):
         value = value + got[k]
     total[...] = value
     columns = pl.ds(pl.multiple_of(tp * cols, cols), cols)
     full[:, columns] = value
-    for k, peer in enumerate(over_tp):
-        begin(
-            functools.partial(remote, total, full.at[:, columns], s2.at[k], r2.at[k], (sp, peer))
-        )
+    for peer in over_tp:
+        remote(total, full.at[:, columns], s2.at[0], r2.at[0], (sp, peer)).start()
+    sent(got.at[pl.ds(0, len(over_tp))], s2.at[0])
     for h in range(upfront, between):
-        begin(functools.partial(over_y, g_own, 0, h))
+        over_y(g_own, 0, h).start()
 
     def rest_own():
         for h in range(between, chunks):
             over_y(g_own, 0, h).start()
-
-    for h in range(between, chunks):
-        drain.append((functools.partial(over_y, g_own, 0, h), None))
 
     @pl.when(same)
     def _():
@@ -444,17 +453,13 @@
         over_y(g_x, 1, h).start()
         to_sib(1, g_x, h).start()
 
-    for h in range(chunks):
-        drain.append((functools.partial(over_y, g_x, 1, h), None))
-        drain.append((functools.partial(to_sib, 1, g_x, h), None))
     relay(0)
     ctx_copy.wait()
     ctx_sib(1 - c).wait_recv()
     for copy in weight_copies + small_copies[3:]:
         copy.wait()
-    for k, peer in enumerate(over_tp):
-        there = pl.ds(pl.multiple_of(peer * cols, cols), cols)
-        remote(total, full.at[:, there], s2.at[k], r2.at[k], (sp, peer)).wait_recv()
+    several = got.at[pl.ds(0, len(over_tp))]
+    remote(several, several, s2.at[0], r2.at[0], sib).wait_recv()
     begin(lambda: remote(wo.at[0], wo.at[1], s_w.at[0], r_w.at[0], sib))
 
     def normed(rows, which):
@@ -515,75 +520,59 @@
                 over_y(g, flow, h).wait_recv()
                 to_sib(k, g, h).start()
 
-    def shared(k, g, cond):
+    def shared(k, g, cond=always, rows=range(own_rows)):
         @pl.when(cond)
         def _():
-            for h in range(chunks):
-                from_sib(k, g, h).wait_recv()
-
-    for h in range(chunks):
-        drain.append((functools.partial(to_sib, 2, g_y, h), None))
-        drain.append((functools.partial(to_sib, 3, g_d, h), None))
+            for r in rows:
+                from_sib(k, g, r).wait_recv()
 
     def before(k):
         if k == 0:
-            for h in range(chunks):
-                from_sib(0, g_own, h).wait_recv()
+            shared(0, g_own)
         if k == 1:
             for h in range(2, chunks):
                 relay(h)
+                if h == chunks - 2:
+                    send_layer(True)
 
             @pl.when(differs)
             def _():
                 rest_own()
 
-            send_layer(True)
             incoming(2, 0, g_y, differs)
-            for h in range(chunks):
-                from_sib(1, g_x, h).wait_recv()
+            shared(1, g_x)
         if k == 2:
             ctx_relay()
-
-            @pl.when(relays & has_down & differs & (g_x == 0))
-            def _():
-                halo_down().start()
-
-            @pl.when(relays & has_up & differs & (g_x == 3))
-            def _():
-                halo_up().start()
-
-            @pl.when(relays & has_down & same & (g_own == 0))
-            def _():
-                halo_down().start()
-
-            @pl.when(relays & has_up & same & (g_own == 3))
-            def _():
-                halo_up().start()
+            for critical, g in ((differs, g_x), (same, g_own)):
+                @pl.when(relays & has_down & critical & (g == 0))
+                def _():
+                    halo_down().start()
+
+                @pl.when(relays & has_up & critical & (g == 3))
+                def _():
+                    halo_up().start()
 
             incoming(3, 1, g_d, same)
             shared(2, g_y, differs)
             shared(3, g_d, same)
-        if k == 3:
-            incoming(2, 0, g_y, same)
-            incoming(3, 1, g_d, differs)
-            shared(2, g_y, same)
-            shared(3, g_d, differs)
+
+    def queries(hidden, count):
+        query = jnp.dot(hidden, wq[...], preferred_element_type=jnp.float32)
+        query = query.reshape(count, GRID_W, cols)
+        query = jnp.concatenate([query[:, GRID_W - half :], query[:, : GRID_W - half]], axis=1)
+        return query.astype(jnp.bfloat16)
 
     def project(i, carry):
-        for k in range(4):
+        for k in range(3):
             @pl.when(i == k)
             def _():
                 before(k)
 
-        g = jnp.where(i == 0, g_own, jnp.where(i == 1, g_x, jnp.where(i == 2, g_third, g_fourth)))
+        g = jnp.where(i == 0, g_own, jnp.where(i == 1, g_x, g_third))
         hidden = jnp.concatenate([normed(buf[2 * g + e], x) for e in range(2)], axis=0)
         value = jnp.dot(hidden, wkv[...], preferred_element_type=jnp.float32).astype(jnp.bfloat16)
         kv[pl.ds(reach + group_rows * g, group_rows)] = value.reshape(group_rows, GRID_W, 2 * cols)
-        query = jnp.dot(hidden, wq[...], preferred_element_type=jnp.float32)
-        query = query.reshape(group_rows, GRID_W, cols)
-        query = jnp.concatenate([query[:, GRID_W - half :], query[:, : GRID_W - half]], axis=1)
-        qs[pl.ds(group_rows * g, group_rows)] = query.astype(jnp.bfloat16)
-
+        qs[pl.ds(group_rows * g, group_rows)] = queries(hidden, group_rows)
         open_now = jnp.logical_not(relays) | (i >= 2)
 
         @pl.when((g == 0) & has_down & open_now)
@@ -596,7 +585,24 @@
 
         return carry
 
-    lax.fori_loop(0, 4, project, 0)
+    lax.fori_loop(0, 3, project, 0)
+
+    def project_row(r, carry):
+        incoming(2, 0, g_y, same & (r == 0))
+        incoming(3, 1, g_d, differs & (r == 0))
+        shared(2, g_y, same, [r])
+        shared(3, g_d, differs, [r])
+        at = pl.ds(pl.multiple_of(GRID_W * r, GRID_W), GRID_W)
+        hidden = jnp.concatenate([normed(buf[2 * g_fourth + e, at], x) for e in range(2)], axis=0)
+        value = jnp.dot(hidden, wkv[...], preferred_element_type=jnp.float32).astype(jnp.bfloat16)
+        query = queries(hidden, 2)
+        for e in range(2):
+            row = group_rows * g_fourth + own_rows * e + r
+            kv[reach + row] = value[GRID_W * e : GRID_W * (e + 1)]
+            qs[row] = query[e]
+        return carry
+
+    lax.fori_loop(0, own_rows, project_row, 0)
     drain.append((halo_down, has_down))
     drain.append((halo_up, has_up))
 
@@ -669,14 +675,14 @@
     def to_across(i, slot, h):
         part_at = pl.ds(pl.multiple_of(h * size, size), size)
         return remote(
-            parts.at[i, part_at], y_in.at[slot, part_at], s_p.at[slot, h], r_p.at[slot, h], across
+            parts.at[i, part_at], y_in.at[slot, part_at], s_p.at[slot], r_p.at[slot, h], across
         )
 
     def chunk(h):
         return pl.ds(pl.multiple_of(h * size, size), size)
 
     def to_owner(h):
-        return remote(fwd.at[chunk(h)], x_in.at[chunk(h)], s_f.at[h], r_f.at[h], beside)
+        return remote(fwd.at[chunk(h)], x_in.at[chunk(h)], s_f.at[0], r_f.at[h], beside)
 
     def sum_at(i, slot, h):
         return parts[i, chunk(h)].astype(jnp.float32) + y_in[slot, chunk(h)].astype(jnp.float32)
@@ -690,7 +696,7 @@
         first = jnp.where(y == 0, 1, 2)
         return jnp.where(i == 0, first, jnp.where(i == 1, 3 * (1 - y), jnp.where(i == 2, g_x, g_own)))
 
-    def attention_block(i, batch, begins, count, between_pairs=None):
+    def attention_block(i, batch, begins, count, between_pairs=None, last_pieces=None):
         g = group_of(i)
         blocks = range(begins // WIN_COLS, (begins + count) // WIN_COLS)
 
@@ -710,6 +716,8 @@
             att[i, pl.ds(own_rows * c, own_rows), at].reshape(own_rows * count, cols), wo[0],
             preferred_element_type=jnp.float32,
         )
+        if last_pieces is not None:
+            last_pieces()
         give(i, batch, begins, count).wait_recv()
         update = acc[: own_rows * count] + jnp.dot(
             att_in[i, :, at].reshape(own_rows * count, cols), wo[1], preferred_element_type=jnp.float32
@@ -719,7 +727,6 @@
                 count * r : count * (r + 1)
             ].astype(jnp.bfloat16)
 
-    per_row = chunks // own_rows
     for part_of in range(2):
         attention_block(0, part_of, GRID_W // 2 * part_of, GRID_W // 2)
         for r in range(own_rows):
@@ -768,8 +775,14 @@
         def _():
             forward(1, early + pair)
 
+    def last_pieces():
+        @pl.when(differs)
+        def _():
+            for h in range(early + pairs, chunks):
+                forward(1, h)
+
     wait_halo(g_own)
-    attention_block(3, 4, 0, GRID_W, between_pairs)
+    attention_block(3, 4, 0, GRID_W, between_pairs, last_pieces)
     for part_of in range(2):
         drain.append((functools.partial(give, 0, part_of, GRID_W // 2 * part_of, GRID_W // 2), None))
     for i in range(1, 4):
@@ -791,8 +804,6 @@
 
     @pl.when(differs)
     def _():
-        for h in range(early + pairs, chunks):
-            forward(1, h)
         own(0)
 
     @pl.when(same)
@@ -802,9 +813,6 @@
     for h in range(chunks):
         to_owner(h).wait_recv()
         finish(1 - x, h, x_in[h * size : (h + 1) * size].astype(jnp.float32))
-        drain.append((functools.partial(to_owner, h), None))
-        for slot in range(2):
-            drain.append((functools.partial(to_across, slot, slot, h), None))
 
     for make, cond in drain:
         if cond is None:
@@ -873,12 +881,12 @@
             pltpu.VMEM((tokens, width), bf16),
             pltpu.VMEM((tokens, width), bf16),
             dma((16,)),
-            dma((n_sp - 1,)), dma((n_sp - 1,)), dma((n_tp - 1,)), dma((n_tp - 1,)),
-            dma((2,)), dma((2,)), dma((chunks,)), dma((chunks,)),
-            dma((2, chunks)), dma((2, chunks)), dma((4, chunks)), dma((4, chunks)),
+            dma((1,)), dma((1,)), dma((1,)), dma((1,)),
+            dma((2,)), dma((2,)), dma((1,)), dma((chunks,)),
+            dma((2,)), dma((2, chunks)), dma((4,)), dma((4, own_rows)),
             dma((6,)), dma((n_z,)), dma((2,)), dma((2,)),
             dma((1,)), dma((1,)), dma((5,)), dma((5,)),
-            dma((2, chunks)), dma((2, chunks)), dma((chunks,)), dma((chunks,)),
+            dma((2,)), dma((2, chunks)), dma((1,)), dma((chunks,)),
         ],
         compiler_params=pltpu.CompilerParams(
             collective_id=1, has_side_effects=True, vmem_limit_bytes=48 * 2**20

time: 70.8 us -> 69.3 us (0.979)
  Pallas kernels: 69.4 us -> 67.9 us
    pallas_call x1, Pallas kernels: 69.4 us -> 67.9 us  [on_eight(): pl.pallas_call(block_kernel, out_shape=jax.ShapeDtypeStruct(latent.shape,...]
where the time goes in v4:
time: 69.3 us; the launch traced here: 69.2 us
  Pallas kernels  67.9 us (98%)
  other arithmetic  1.26 us (2%)
    pallas_call x1, Pallas kernels, on_eight(): pl.pallas_call(block_kernel, out_shape=jax.ShapeDtypeStruct(latent.shape,...  67.9 us

profile of v4, /device:TPU:0, one launch (start us, length us, event | category | flops | bytes accessed | tf_op | source)
XLA Modules:
  0.0 69.2 jit_solution(9752566273233813675)
XLA Ops:
  0.0 0.0 copy-start
  0.0 67.9 %shard_map.136 = f32[2,128,2048]{2,1,0:T(8,128)S(1)} custom-call(f32[8]{0:T(128)} %far_hbm.1, f32[15,8,31]{2,1,0:T(8,128)} %bitcast.3, f32[1,2048]{1,0:T(1,128)} %bitcast.4, bf16[2,2048]{1,0:T(2,128)(2,1)} %cond_hbm.1, bf16[16,128]{1,0:T(8,128)(2,1)} %bitcast.5, bf16[256,512]{1,0:T(8,128)(2,1)} %ws_ref.1, bf16[256,512]{1,0:T(8,128)(2,1)} %wc_ref.1, ...), custom_call_target="tpu_custom_call" | custom-call | tf_op jit(solution)/shard_map/pallas_call | solution.py:847
  67.9 0.0 copy-done
  67.9 1.3 %add_convert_fusion = bf16[2,128,2048]{2,1,0:T(8,128)(2,1)} fusion(f32[2,128,2048]{2,1,0:T(8,128)S(1)} %shard_map.136, bf16[2,128,2048]{2,1,0:T(8,128)(2,1)S(1)} %copy-done), kind=kLoop, calls=%fused_computation | loop fusion | flops 1572864 | bytes 4194304 | tf_op jit(solution)/shard_map/convert_element_type | solution.py:903
Async XLA Ops:
  0.0 67.9 %copy-start = (bf16[2,128,2048]{2,1,0:T(8,128)(2,1)S(1)}, bf16[2,128,2048]{2,1,0:T(8,128)(2,1)}, u32[]{:S(2)}) copy-start(bf16[2,128,2048]{2,1,0:T(8,128)(2,1)} %latent_ref.1) | copy-start | bytes 3145732

commit v5 on v4

--- a/solution.py
+++ b/solution.py
@@ -453,7 +453,6 @@
         over_y(g_x, 1, h).start()
         to_sib(1, g_x, h).start()
 
-    relay(0)
     ctx_copy.wait()
     ctx_sib(1 - c).wait_recv()
     for copy in weight_copies + small_copies[3:]:
@@ -488,6 +487,7 @@
                 make().start()
 
     send_layer(False)
+    relay(0)
     relay(1)
     far_up, far_down = z == n_z - 2, z == 1
     relays = far_up | far_down

time: 69.3 us -> 69.3 us (level)
  no operation moved by 1% of the time
where the time goes in v5:
time: 69.3 us; the launch traced here: 69.2 us
  Pallas kernels  67.9 us (98%)
  other arithmetic  1.26 us (2%)
    pallas_call x1, Pallas kernels, on_eight(): pl.pallas_call(block_kernel, out_shape=jax.ShapeDtypeStruct(latent.shape,...  67.9 us

profile of v5, /device:TPU:0, one launch (start us, length us, event | category | flops | bytes accessed | tf_op | source)
XLA Modules:
  0.0 69.2 jit_solution(6177697188115047773)
XLA Ops:
  0.0 0.0 copy-start
  0.0 67.9 %shard_map.136 = f32[2,128,2048]{2,1,0:T(8,128)S(1)} custom-call(f32[8]{0:T(128)} %far_hbm.1, f32[15,8,31]{2,1,0:T(8,128)} %bitcast.3, f32[1,2048]{1,0:T(1,128)} %bitcast.4, bf16[2,2048]{1,0:T(2,128)(2,1)} %cond_hbm.1, bf16[16,128]{1,0:T(8,128)(2,1)} %bitcast.5, bf16[256,512]{1,0:T(8,128)(2,1)} %ws_ref.1, bf16[256,512]{1,0:T(8,128)(2,1)} %wc_ref.1, ...), custom_call_target="tpu_custom_call" | custom-call | tf_op jit(solution)/shard_map/pallas_call | solution.py:847
  67.9 0.0 copy-done
  67.9 1.3 %add_convert_fusion = bf16[2,128,2048]{2,1,0:T(8,128)(2,1)} fusion(f32[2,128,2048]{2,1,0:T(8,128)S(1)} %shard_map.136, bf16[2,128,2048]{2,1,0:T(8,128)(2,1)S(1)} %copy-done), kind=kLoop, calls=%fused_computation | loop fusion | flops 1572864 | bytes 4194304 | tf_op jit(solution)/shard_map/convert_element_type | solution.py:903
Async XLA Ops:
  0.0 67.9 %copy-start = (bf16[2,128,2048]{2,1,0:T(8,128)(2,1)S(1)}, bf16[2,128,2048]{2,1,0:T(8,128)(2,1)}, u32[]{:S(2)}) copy-start(bf16[2,128,2048]{2,1,0:T(8,128)(2,1)} %latent_ref.1) | copy-start | bytes 3145732
